TPU v7x, 256 devices: a 4x2x16 block of a 4x16x16 slice. The times are simulated.
256 devices in a mesh: grp: 2 (over y), ra: 16 (over z), cb: 4 (over x), dp: 2 (over core).
Axes of the slice: x: 4, y: 2, z: 16, core: 2. Of those that a mesh axis runs over, the one named last changes fastest.
The devices are a block of a 4x16x16 slice.
Arguments:
- tokens: bfloat16 [256, 2048], P(('grp', 'dp'), 'ra'), parts along dimension 0, may hold values from -62 to 62
- gain_first: float32 [2048], P('ra'), may hold values from 0.1 to 1.9
- up_first: bfloat16 [2048, 8192], P('ra', 'cb'), may hold values from -0.125 to 0.125
- down_first: bfloat16 [8192, 2048], P('cb', 'ra'), may hold values from -0.0625 to 0.0625
- gain_second: float32 [2048], P('ra'), may hold values from 0.1 to 1.9
- up_second: bfloat16 [2048, 8192], P('ra', 'cb'), may hold values from -0.125 to 0.125
- down_second: bfloat16 [8192, 2048], P('cb', 'ra'), may hold values from -0.0625 to 0.0625
- gain_last: float32 [2048], P('ra'), may hold values from 0.1 to 1.9
Outputs:
- normed: bfloat16 [256, 2048], P(('grp', 'dp'), 'ra'), parts along dimension 0
There are 2 independent parts, one for each index of `grp`. A program takes and returns all parts, laid end to end along the dimension named above; an argument that names none is the same for every part. Nothing has to cross between parts.
All inputs are finite; a program needn't handle non-finite values.
Results may differ from a plain program's by a relative error of at most 0.0095.
Values may be sent and summed in bfloat16 or wider, within the bound.
No kernel may reach another device: no remote copies, remote signals or barrier semaphores. Data moves between devices by JAX's collectives and lax.ppermute only.
A program may use at most 64 MiB of HBM per device.

v0:
```python
import jax
import jax.numpy as jnp
from jax import lax
from jax.sharding import PartitionSpec as P

D = 2048


EPS = 1e-06


def sent_to_all(shard, axis):
    copies = jnp.broadcast_to(shard, (lax.axis_size(axis), *shard.shape))
    return lax.all_to_all(copies, axis, split_axis=0, concat_axis=0, tiled=True)


def over_copies(shard, axis):
    return sent_to_all(shard, axis).sum(axis=0)


def split_up(shard, dim, size):
    shape = shard.shape
    pieces = shard.reshape(*shape[:dim], size, shape[dim] // size, *shape[dim + 1 :])
    return jnp.moveaxis(pieces, dim, 0)


def summed_on_arrival(shard, axis, dim):
    pieces = split_up(shard, dim, lax.axis_size(axis))
    arrived = lax.all_to_all(pieces, axis, split_axis=0, concat_axis=0, tiled=True)
    return arrived.sum(axis=0)


def in_order(pieces, dim):
    shape = list(pieces.shape[1:])
    shape[dim] *= pieces.shape[0]
    return jnp.moveaxis(pieces, 0, dim).reshape(shape)


def gathered_copies(shard, axis, dim):
    pieces = sent_to_all(shard, axis)
    return in_order(pieces, dim)


def squares_inverse(h32):
    local_sq = jnp.sum(h32 * h32, axis=1)
    summed_sq = over_copies(local_sq, "ra")
    return lax.rsqrt(summed_sq / D + EPS)


def activate(summed, inverse):
    return jnp.square(jax.nn.relu(summed * inverse[:, None])).astype(jnp.bfloat16)


def mlp_branch(h32, gain, w_up, w_down):
    scaled = (h32 * gain).astype(jnp.bfloat16)
    partial_value = jnp.dot(scaled, w_up, preferred_element_type=jnp.float32)
    inverse = squares_inverse(h32)
    shared = summed_on_arrival(partial_value, "ra", 1)
    hidden_share = activate(shared, inverse)
    down = jnp.dot(
        gathered_copies(hidden_share, "ra", 1), w_down, preferred_element_type=jnp.float32
    )
    return over_copies(down, "cb")


def local(tokens, gain_first, up_first, down_first, gain_second, up_second, down_second, gain_last):
    start32 = tokens.astype(jnp.float32)
    first = (0.5 * start32 + mlp_branch(start32, gain_first, up_first, down_first)).astype(
        jnp.bfloat16
    )
    first32 = first.astype(jnp.float32)
    second = (0.5 * first32 + mlp_branch(first32, gain_second, up_second, down_second)).astype(
        jnp.bfloat16
    )
    second32 = second.astype(jnp.float32)
    inverse = squares_inverse(second32)
    return (second32 * inverse[:, None] * gain_last).astype(jnp.bfloat16)


def solution(mesh):
    return jax.shard_map(
        local,
        mesh=mesh,
        in_specs=(
            P(("grp", "dp"), "ra"),
            P("ra"),
            P("ra", "cb"),
            P("cb", "ra"),
            P("ra"),
            P("ra", "cb"),
            P("cb", "ra"),
            P("ra"),
        ),
        out_specs=P(("grp", "dp"), "ra"),
        check_vma=False,
    )
```

profile of v0, /device:TPU:33, one launch (start us, length us, event | category | flops | bytes accessed | tf_op | source)
XLA Modules:
  0.0 202.9 jit_solution(14024609019446180405)
XLA Ops:
  0.0 0.9 fusion.12
  0.9 0.6 broadcast_in_dim.27
  1.5 24.6 %all-to-all-start.1 = ((f32[16,1,64]{2,1,0:T(1,128)}), f32[16,1,64]{2,1,0:T(1,128)S(1)}, u32[]{:S(2)}, u32[]{:S(2)}) async-start(f32[16,1,64]{2,1,0:T(1,128)} %broadcast_in_dim.27), calls=%async_computation.1 | async-start | bytes 16384 | tf_op jit(solution)/shard_map/all_to_all | solution.py:14
  26.2 0.2 convolution_bitcast_fusion.1
  26.4 0.8 copy.39
  27.3 10.0 %all-to-all-done.1 = f32[16,1,64]{2,1,0:T(1,128)S(1)} async-done(((f32[16,1,64]{2,1,0:T(1,128)}), f32[16,1,64]{2,1,0:T(1,128)S(1)}, u32[]{:S(2)}, u32[]{:S(2)}) %all-to-all-start.1) | async-done | bytes 4128 | tf_op jit(solution)/shard_map/all_to_all | solution.py:14
  37.2 4.0 %all-to-all-start = ((f32[16,64,128]{2,1,0:T(8,128)}), f32[16,64,128]{2,1,0:T(8,128)S(1)}, u32[]{:S(2)}, u32[]{:S(2)}) async-start(f32[16,64,128]{2,1,0:T(8,128)} %bitcast.38), calls=%async_computation | async-start | bytes 1048576 | tf_op jit(solution)/shard_map/all_to_all | solution.py:29
  41.3 22.7 %all-to-all-done = f32[16,64,128]{2,1,0:T(8,128)S(1)} async-done(((f32[16,64,128]{2,1,0:T(8,128)}), f32[16,64,128]{2,1,0:T(8,128)S(1)}, u32[]{:S(2)}, u32[]{:S(2)}) %all-to-all-start) | async-done | bytes 524320 | tf_op jit(solution)/shard_map/all_to_all | solution.py:29
  64.2 25.2 %all_to_all.48 = bf16[16,64,128]{2,1,0:T(8,128)(2,1)S(1)} all-to-all(bf16[16,64,128]{2,1,0:T(8,128)(2,1)S(1)} %broadcast_in_dim.28), channel_id=1, replica_groups=mesh['grp'=2,'ra'=16,'cb'=4,'dp'=2] {'ra'}, dimensions={0} | all-to-all | bytes 524288 | tf_op jit(solution)/shard_map/all_to_all | solution.py:14
  89.4 0.2 fusion.3
  89.6 9.1 %all_to_all.49 = f32[4,64,128]{2,1,0:T(8,128)S(1)} all-to-all(f32[4,64,128]{2,1,0:T(8,128)S(1)} %broadcast_in_dim.29), channel_id=1, replica_groups=mesh['grp'=2,'ra'=16,'cb'=4,'dp'=2] {'cb'}, dimensions={0} | all-to-all | bytes 262144 | tf_op jit(solution)/shard_map/all_to_all | solution.py:14
  98.8 0.6 broadcast_in_dim.30
  99.4 11.1 %all-to-all-start.5 = ((f32[16,1,64]{2,1,0:T(1,128)}), f32[16,1,64]{2,1,0:T(1,128)S(1)}, u32[]{:S(2)}, u32[]{:S(2)}) async-start(f32[16,1,64]{2,1,0:T(1,128)} %broadcast_in_dim.30), calls=%async_computation.5 | async-start | bytes 16384 | tf_op jit(solution)/shard_map/all_to_all | solution.py:14
  110.6 0.6 copy-done.6
  111.4 0.8 copy.38
  112.3 9.3 %all-to-all-done.5 = f32[16,1,64]{2,1,0:T(1,128)S(1)} async-done(((f32[16,1,64]{2,1,0:T(1,128)}), f32[16,1,64]{2,1,0:T(1,128)S(1)}, u32[]{:S(2)}, u32[]{:S(2)}) %all-to-all-start.5) | async-done | bytes 4128 | tf_op jit(solution)/shard_map/all_to_all | solution.py:14
  121.6 4.0 %all-to-all-start.4 = ((f32[16,64,128]{2,1,0:T(8,128)}), f32[16,64,128]{2,1,0:T(8,128)S(1)}, u32[]{:S(2)}, u32[]{:S(2)}) async-start(f32[16,64,128]{2,1,0:T(8,128)} %bitcast.36), calls=%async_computation.4 | async-start | bytes 1048576 | tf_op jit(solution)/shard_map/all_to_all | solution.py:29
  125.7 22.2 %all-to-all-done.4 = f32[16,64,128]{2,1,0:T(8,128)S(1)} async-done(((f32[16,64,128]{2,1,0:T(8,128)}), f32[16,64,128]{2,1,0:T(8,128)S(1)}, u32[]{:S(2)}, u32[]{:S(2)}) %all-to-all-start.4) | async-done | bytes 524320 | tf_op jit(solution)/shard_map/all_to_all | solution.py:29
  148.1 24.4 %all_to_all.50 = bf16[16,64,128]{2,1,0:T(8,128)(2,1)S(1)} all-to-all(bf16[16,64,128]{2,1,0:T(8,128)(2,1)S(1)} %broadcast_in_dim.31), channel_id=1, replica_groups=mesh['grp'=2,'ra'=16,'cb'=4,'dp'=2] {'ra'}, dimensions={0} | all-to-all | bytes 524288 | tf_op jit(solution)/shard_map/all_to_all | solution.py:14
  172.5 0.2 fusion
  172.7 7.2 %all_to_all.51 = f32[4,64,128]{2,1,0:T(8,128)S(1)} all-to-all(f32[4,64,128]{2,1,0:T(8,128)S(1)} %broadcast_in_dim.32), channel_id=1, replica_groups=mesh['grp'=2,'ra'=16,'cb'=4,'dp'=2] {'cb'}, dimensions={0} | all-to-all | bytes 262144 | tf_op jit(solution)/shard_map/all_to_all | solution.py:14
  180.1 21.4 %all_to_all.52 = f32[16,1,64]{2,1,0:T(1,128)S(1)} all-to-all(f32[16,1,64]{2,1,0:T(1,128)S(1)} %broadcast_in_dim.33), channel_id=1, replica_groups=mesh['grp'=2,'ra'=16,'cb'=4,'dp'=2] {'ra'}, dimensions={0} | all-to-all | bytes 8192 | tf_op jit(solution)/shard_map/all_to_all | solution.py:14
  201.6 0.6 copy-done.7
  202.2 0.7 fusion.8
  (34 shorter events, 0.9 us)
Async XLA Ops:
  0.0 26.2 %copy-start = (bf16[128,2048]{1,0:T(8,128)(2,1)S(1)}, bf16[128,2048]{1,0:T(8,128)(2,1)}, u32[]{:S(2)}) copy-start(bf16[128,2048]{1,0:T(8,128)(2,1)} %param.10) | copy-start | bytes 1572868
  0.9 25.3 %copy-start.4 = (bf16[64,128]{1,0:T(8,128)(2,1)S(1)}, bf16[64,128]{1,0:T(8,128)(2,1)}, u32[]{:S(2)}) copy-start(bf16[64,128]{1,0:T(8,128)(2,1)} %param.8) | copy-start | bytes 49156
  1.5 24.7 %copy-start.5 = (f32[128]{0:T(128)S(1)}, f32[128]{0:T(128)}, u32[]{:S(2)}) copy-start(f32[128]{0:T(128)} %param.9) | copy-start | bytes 1540
  1.5 35.7 %all-to-all-start.1 = ((f32[16,1,64]{2,1,0:T(1,128)}), f32[16,1,64]{2,1,0:T(1,128)S(1)}, u32[]{:S(2)}, u32[]{:S(2)}) async-start(f32[16,1,64]{2,1,0:T(1,128)} %broadcast_in_dim.27), calls=%async_computation.1 | async-start | bytes 16384 | tf_op jit(solution)/shard_map/all_to_all | solution.py:14
  37.2 26.8 %all-to-all-start = ((f32[16,64,128]{2,1,0:T(8,128)}), f32[16,64,128]{2,1,0:T(8,128)S(1)}, u32[]{:S(2)}, u32[]{:S(2)}) async-start(f32[16,64,128]{2,1,0:T(8,128)} %bitcast.38), calls=%async_computation | async-start | bytes 1048576 | tf_op jit(solution)/shard_map/all_to_all | solution.py:29
  64.0 25.4 %copy-start.1 = (bf16[2048,128]{1,0:T(8,128)(2,1)S(1)}, bf16[2048,128]{1,0:T(8,128)(2,1)}, u32[]{:S(2)}) copy-start(bf16[2048,128]{1,0:T(8,128)(2,1)} %param.11) | copy-start | bytes 1572868
  89.6 21.0 %copy-start.3 = (bf16[128,2048]{1,0:T(8,128)(2,1)S(1)}, bf16[128,2048]{1,0:T(8,128)(2,1)}, u32[]{:S(2)}) copy-start(bf16[128,2048]{1,0:T(8,128)(2,1)} %param.13) | copy-start | bytes 1572868
  99.4 22.2 %all-to-all-start.5 = ((f32[16,1,64]{2,1,0:T(1,128)}), f32[16,1,64]{2,1,0:T(1,128)S(1)}, u32[]{:S(2)}, u32[]{:S(2)}) async-start(f32[16,1,64]{2,1,0:T(1,128)} %broadcast_in_dim.30), calls=%async_computation.5 | async-start | bytes 16384 | tf_op jit(solution)/shard_map/all_to_all | solution.py:14
  110.6 0.7 copy-start.6
  121.6 26.3 %all-to-all-start.4 = ((f32[16,64,128]{2,1,0:T(8,128)}), f32[16,64,128]{2,1,0:T(8,128)S(1)}, u32[]{:S(2)}, u32[]{:S(2)}) async-start(f32[16,64,128]{2,1,0:T(8,128)} %bitcast.36), calls=%async_computation.4 | async-start | bytes 1048576 | tf_op jit(solution)/shard_map/all_to_all | solution.py:29
  147.9 24.5 %copy-start.2 = (bf16[2048,128]{1,0:T(8,128)(2,1)S(1)}, bf16[2048,128]{1,0:T(8,128)(2,1)}, u32[]{:S(2)}) copy-start(bf16[2048,128]{1,0:T(8,128)(2,1)} %param.14) | copy-start | bytes 1572868
  201.6 0.7 copy-start.7
where the time goes:
time: 207 us; the launch traced here: 203 us
  blocking collectives  87.4 us (42%)
  waiting for transfers between devices  64.2 us (31%)
  starting transfers between devices  43.8 us (21%)
  local copies, waits for them, and re-layouts  4.34 us (2%)
  other arithmetic  2.1 us (1%)
    all_to_all x5, blocking collectives, sent_to_all(): return lax.all_to_all(copies, axis, split_axis=0, concat_axis=0, tiled=True)  87.4 us
    all_to_all x2, waiting for transfers between devices, summed_on_arrival(): lax.all_to_all(pieces, axis, split_axis=0, concat_axis=0, tiled=True)  45 us
    all_to_all x2, starting transfers between devices, sent_to_all(): return lax.all_to_all(copies, axis, split_axis=0, concat_axis=0, tiled=True)  35.7 us
    all_to_all x2, waiting for transfers between devices, sent_to_all(): return lax.all_to_all(copies, axis, split_axis=0, concat_axis=0, tiled=True)  19.3 us
    all_to_all x2, starting transfers between devices, summed_on_arrival(): lax.all_to_all(pieces, axis, split_axis=0, concat_axis=0, tiled=True)  8.03 us
  transfers between devices with their start and end apart: 4, of which 4 were waited for; matrix products, arithmetic and copies ran while one was open for 1% of the time, Pallas kernels for 0%

commit v1 on v0

v1 whole, which is shorter than its diff:
```python
import jax
import jax.numpy as jnp
from jax import lax
from jax.sharding import PartitionSpec as P

EPS = 1e-06
F32 = jnp.float32
BF16 = jnp.bfloat16


def exchange(pieces, axis):
    return lax.all_to_all(pieces, axis, split_axis=0, concat_axis=0, tiled=True)


def sent_to_all(shard, axis):
    return exchange(jnp.broadcast_to(shard, (lax.axis_size(axis), *shard.shape)), axis)


def local_squares(h32):
    return jnp.sum(h32 * h32, axis=1)


def packed_row(values):
    high = lax.reduce_precision(values, 8, 7)
    row = jnp.concatenate([high, values - high])[None, :]
    return jnp.pad(row, ((0, 7), (0, 0))).astype(BF16)


def mlp_branch(h32, gain, w_up, w_down):
    rows, lanes = h32.shape
    ra = lax.axis_size("ra")
    scaled = (h32 * gain).astype(BF16)
    partial_value = jnp.dot(scaled, w_up, preferred_element_type=F32).astype(BF16)
    pieces = jnp.moveaxis(partial_value.reshape(rows, ra, -1), 1, 0)
    shared = exchange(pieces, "ra").astype(F32).sum(axis=0)
    hidden_share = jnp.square(jax.nn.relu(shared)).astype(BF16)
    share = jnp.concatenate([hidden_share, packed_row(local_squares(h32))], axis=0)
    everyone = sent_to_all(share, "ra")
    hidden = jnp.moveaxis(everyone[:, :rows], 0, 1).reshape(rows, -1)
    squares = everyone[:, rows].astype(F32).sum(axis=0)
    mean_sq = (squares[:rows] + squares[rows:]) / (ra * lanes)
    down = jnp.dot(hidden, w_down, preferred_element_type=F32)
    return sent_to_all(down, "cb").sum(axis=0) / (mean_sq + EPS)[:, None]


def local(tokens, gain_first, up_first, down_first, gain_second, up_second, down_second, gain_last):
    start32 = tokens.astype(F32)
    first = (0.5 * start32 + mlp_branch(start32, gain_first, up_first, down_first)).astype(BF16)
    first32 = first.astype(F32)
    second = (0.5 * first32 + mlp_branch(first32, gain_second, up_second, down_second)).astype(BF16)
    second32 = second.astype(F32)
    squares = sent_to_all(local_squares(second32), "ra").sum(axis=0)
    inverse = lax.rsqrt(squares / (lax.axis_size("ra") * second.shape[1]) + EPS)
    return (second32 * inverse[:, None] * gain_last).astype(BF16)


def solution(mesh):
    return jax.shard_map(
        local,
        mesh=mesh,
        in_specs=(
            P(("grp", "dp"), "ra"),
            P("ra"),
            P("ra", "cb"),
            P("cb", "ra"),
            P("ra"),
            P("ra", "cb"),
            P("cb", "ra"),
            P("ra"),
        ),
        out_specs=P(("grp", "dp"), "ra"),
        check_vma=False,
    )
```

time: 207 us -> 162 us (0.78)
  waiting for transfers between devices: 64.2 us -> 35.1 us
  blocking collectives: 87.4 us -> 71.3 us
    all_to_all x4, waiting for transfers between devices: 64.2 us -> 35.1 us  [exchange(): return lax.all_to_all(pieces, axis, split_axis=0, concat_axis=0, tiled=True)]
    all_to_all x5 -> x3, blocking collectives: 87.4 us -> 71.3 us  [exchange(): return lax.all_to_all(pieces, axis, split_axis=0, concat_axis=0, tiled=True)]
  transfers between devices with their start and end apart: 4 -> 4, of which waited for: 4 -> 4; matrix products, arithmetic and copies ran while one was open for 1% -> 0% of each run, Pallas kernels for 0% -> 0%
where the time goes in v1:
time: 162 us; the launch traced here: 159 us
  blocking collectives  71.3 us (44%)
  starting transfers between devices  43.9 us (27%)
  waiting for transfers between devices  35.1 us (22%)
  local copies, waits for them, and re-layouts  5.27 us (3%)
  other arithmetic  1.71 us (1%)
    all_to_all x3, blocking collectives, exchange(): return lax.all_to_all(pieces, axis, split_axis=0, concat_axis=0, tiled=True)  71.3 us
    all_to_all x4, starting transfers between devices, exchange(): return lax.all_to_all(pieces, axis, split_axis=0, concat_axis=0, tiled=True)  43.9 us
    all_to_all x4, waiting for transfers between devices, exchange(): return lax.all_to_all(pieces, axis, split_axis=0, concat_axis=0, tiled=True)  35.1 us
  transfers between devices with their start and end apart: 4, of which 4 were waited for; matrix products, arithmetic and copies ran while one was open for 0% of the time, Pallas kernels for 0%

profile of v1, /device:TPU:33, one launch (start us, length us, event | category | flops | bytes accessed | tf_op | source)
XLA Modules:
  0.0 159.1 jit_solution(2969009121592865426)
XLA Ops:
  0.0 1.0 copy-done
  1.0 0.9 fusion
  2.0 0.8 copy.37
  2.8 24.6 %all-to-all-start = ((bf16[16,64,128]{2,1,0:T(8,128)(2,1)}), bf16[16,64,128]{2,1,0:T(8,128)(2,1)S(1)}, u32[]{:S(2)}, u32[]{:S(2)}) async-start(bf16[16,64,128]{2,1,0:T(8,128)(2,1)} %bitcast.40), calls=%async_computation | async-start | bytes 524288 | tf_op jit(solution)/shard_map/all_to_all | solution.py:12
  27.6 13.4 %all-to-all-done = bf16[16,64,128]{2,1,0:T(8,128)(2,1)S(1)} async-done(((bf16[16,64,128]{2,1,0:T(8,128)(2,1)}), bf16[16,64,128]{2,1,0:T(8,128)(2,1)S(1)}, u32[]{:S(2)}, u32[]{:S(2)}) %all-to-all-start) | async-done | bytes 262176 | tf_op jit(solution)/shard_map/all_to_all | solution.py:12
  41.1 24.4 %all_to_all.36 = bf16[16,72,128]{2,1,0:T(8,128)(2,1)S(1)} all-to-all(bf16[16,72,128]{2,1,0:T(8,128)(2,1)S(1)} %broadcast_in_dim.30), channel_id=1, replica_groups=mesh['grp'=2,'ra'=16,'cb'=4,'dp'=2] {'ra'}, dimensions={0} | all-to-all | bytes 589824 | tf_op jit(solution)/shard_map/all_to_all | solution.py:12
  65.5 0.2 fusion.5
  65.8 0.6 broadcast_in_dim.31
  66.4 4.3 %all-to-all-start.2 = ((f32[4,64,128]{2,1,0:T(8,128)}), f32[4,64,128]{2,1,0:T(8,128)S(1)}, u32[]{:S(2)}, u32[]{:S(2)}) async-start(f32[4,64,128]{2,1,0:T(8,128)} %broadcast_in_dim.31), calls=%async_computation.2 | async-start | bytes 262144 | tf_op jit(solution)/shard_map/all_to_all | solution.py:12
  70.8 4.7 %all-to-all-done.2 = f32[4,64,128]{2,1,0:T(8,128)S(1)} async-done(((f32[4,64,128]{2,1,0:T(8,128)}), f32[4,64,128]{2,1,0:T(8,128)S(1)}, u32[]{:S(2)}, u32[]{:S(2)}) %all-to-all-start.2) | async-done | bytes 131104 | tf_op jit(solution)/shard_map/all_to_all | solution.py:12
  75.6 0.2 fusion.20
  75.8 0.6 copy-done.6
  76.4 0.2 fusion.1
  76.6 0.8 copy.36
  77.4 11.5 %all-to-all-start.3 = ((bf16[16,64,128]{2,1,0:T(8,128)(2,1)}), bf16[16,64,128]{2,1,0:T(8,128)(2,1)S(1)}, u32[]{:S(2)}, u32[]{:S(2)}) async-start(bf16[16,64,128]{2,1,0:T(8,128)(2,1)} %bitcast.38), calls=%async_computation.3 | async-start | bytes 524288 | tf_op jit(solution)/shard_map/all_to_all | solution.py:12
  89.0 12.4 %all-to-all-done.3 = bf16[16,64,128]{2,1,0:T(8,128)(2,1)S(1)} async-done(((bf16[16,64,128]{2,1,0:T(8,128)(2,1)}), bf16[16,64,128]{2,1,0:T(8,128)(2,1)S(1)}, u32[]{:S(2)}, u32[]{:S(2)}) %all-to-all-start.3) | async-done | bytes 262176 | tf_op jit(solution)/shard_map/all_to_all | solution.py:12
  101.6 23.9 %all_to_all.37 = bf16[16,72,128]{2,1,0:T(8,128)(2,1)S(1)} all-to-all(bf16[16,72,128]{2,1,0:T(8,128)(2,1)S(1)} %broadcast_in_dim.33), channel_id=1, replica_groups=mesh['grp'=2,'ra'=16,'cb'=4,'dp'=2] {'ra'}, dimensions={0} | all-to-all | bytes 589824 | tf_op jit(solution)/shard_map/all_to_all | solution.py:12
  125.5 0.2 fusion.2
  125.7 0.6 broadcast_in_dim.34
  126.4 3.4 %all-to-all-start.5 = ((f32[4,64,128]{2,1,0:T(8,128)}), f32[4,64,128]{2,1,0:T(8,128)S(1)}, u32[]{:S(2)}, u32[]{:S(2)}) async-start(f32[4,64,128]{2,1,0:T(8,128)} %broadcast_in_dim.34), calls=%async_computation.5 | async-start | bytes 262144 | tf_op jit(solution)/shard_map/all_to_all | solution.py:12
  129.9 4.6 %all-to-all-done.5 = f32[4,64,128]{2,1,0:T(8,128)S(1)} async-done(((f32[4,64,128]{2,1,0:T(8,128)}), f32[4,64,128]{2,1,0:T(8,128)S(1)}, u32[]{:S(2)}, u32[]{:S(2)}) %all-to-all-start.5) | async-done | bytes 131104 | tf_op jit(solution)/shard_map/all_to_all | solution.py:12
  134.8 23.0 %all_to_all.38 = f32[16,1,64]{2,1,0:T(1,128)S(1)} all-to-all(f32[16,1,64]{2,1,0:T(1,128)S(1)} %broadcast_in_dim.35), channel_id=1, replica_groups=mesh['grp'=2,'ra'=16,'cb'=4,'dp'=2] {'ra'}, dimensions={0} | all-to-all | bytes 8192 | tf_op jit(solution)/shard_map/all_to_all | solution.py:12
  157.8 0.7 copy-done.5
  158.4 0.7 fusion.12
  (34 shorter events, 1.0 us)
Async XLA Ops:
  0.0 1.0 copy-start
  2.7 24.7 %copy-start.4 = (bf16[64,128]{1,0:T(8,128)(2,1)S(1)}, bf16[64,128]{1,0:T(8,128)(2,1)}, u32[]{:S(2)}) copy-start(bf16[64,128]{1,0:T(8,128)(2,1)} %param.8) | copy-start | bytes 49156
  2.8 38.2 %all-to-all-start = ((bf16[16,64,128]{2,1,0:T(8,128)(2,1)}), bf16[16,64,128]{2,1,0:T(8,128)(2,1)S(1)}, u32[]{:S(2)}, u32[]{:S(2)}) async-start(bf16[16,64,128]{2,1,0:T(8,128)(2,1)} %bitcast.40), calls=%async_computation | async-start | bytes 524288 | tf_op jit(solution)/shard_map/all_to_all | solution.py:12
  41.0 24.5 %copy-start.1 = (bf16[2048,128]{1,0:T(8,128)(2,1)S(1)}, bf16[2048,128]{1,0:T(8,128)(2,1)}, u32[]{:S(2)}) copy-start(bf16[2048,128]{1,0:T(8,128)(2,1)} %param.11) | copy-start | bytes 1572868
  65.8 10.0 %copy-start.2 = (bf16[128,2048]{1,0:T(8,128)(2,1)S(1)}, bf16[128,2048]{1,0:T(8,128)(2,1)}, u32[]{:S(2)}) copy-start(bf16[128,2048]{1,0:T(8,128)(2,1)} %param.13) | copy-start | bytes 1572868
  66.4 9.1 %all-to-all-start.2 = ((f32[4,64,128]{2,1,0:T(8,128)}), f32[4,64,128]{2,1,0:T(8,128)S(1)}, u32[]{:S(2)}, u32[]{:S(2)}) async-start(f32[4,64,128]{2,1,0:T(8,128)} %broadcast_in_dim.31), calls=%async_computation.2 | async-start | bytes 262144 | tf_op jit(solution)/shard_map/all_to_all | solution.py:12
  75.7 0.7 copy-start.6
  77.4 24.0 %all-to-all-start.3 = ((bf16[16,64,128]{2,1,0:T(8,128)(2,1)}), bf16[16,64,128]{2,1,0:T(8,128)(2,1)S(1)}, u32[]{:S(2)}, u32[]{:S(2)}) async-start(bf16[16,64,128]{2,1,0:T(8,128)(2,1)} %bitcast.38), calls=%async_computation.3 | async-start | bytes 524288 | tf_op jit(solution)/shard_map/all_to_all | solution.py:12
  101.5 24.0 %copy-start.3 = (bf16[2048,128]{1,0:T(8,128)(2,1)S(1)}, bf16[2048,128]{1,0:T(8,128)(2,1)}, u32[]{:S(2)}) copy-start(bf16[2048,128]{1,0:T(8,128)(2,1)} %param.14) | copy-start | bytes 1572868
  126.4 8.2 %all-to-all-start.5 = ((f32[4,64,128]{2,1,0:T(8,128)}), f32[4,64,128]{2,1,0:T(8,128)S(1)}, u32[]{:S(2)}, u32[]{:S(2)}) async-start(f32[4,64,128]{2,1,0:T(8,128)} %broadcast_in_dim.34), calls=%async_computation.5 | async-start | bytes 262144 | tf_op jit(solution)/shard_map/all_to_all | solution.py:12
  157.7 0.7 copy-start.5

commit v2 on v1

v2 whole, which is shorter than its diff:
```python
import jax
import jax.numpy as jnp
from jax import lax
from jax.experimental import pallas as pl
from jax.experimental.pallas import tpu as pltpu
from jax.sharding import PartitionSpec as P

EPS = 1e-06
F32 = jnp.float32
BF16 = jnp.bfloat16
STAGGER_NS = 13000
STAGGER_CORE = 1
UP_COST = 2 << 20


def exchange(pieces, axis):
    return lax.all_to_all(pieces, axis, split_axis=0, concat_axis=0, tiled=True)


def sent_to_all(shard, axis):
    return exchange(jnp.broadcast_to(shard, (lax.axis_size(axis), *shard.shape)), axis)


def summed_over(value, axis):
    size = lax.axis_size(axis)
    total = value
    for step in range(1, size):
        total = total + lax.ppermute(value, axis, [(i, (i + step) % size) for i in range(size)])
    return total


def packed_row(h32):
    sums = jnp.sum(h32 * h32, axis=1)
    high = lax.reduce_precision(sums, 8, 7)
    row = jnp.stack([high, sums - high])
    return jnp.pad(row, ((0, 6), (0, h32.shape[1] - sums.shape[0]))).astype(BF16)


def write_pieces(scaled, up_ref, pieces_ref, piece):
    width = pieces_ref.shape[2]
    lanes = pl.ds(piece * width, width)
    pieces_ref[piece] = jnp.dot(scaled, up_ref[:, lanes], preferred_element_type=F32).astype(BF16)


def write_squares(h32, squares_ref):
    sums = jnp.sum(jnp.transpose(h32 * h32), axis=0, keepdims=True)
    rows = sums.shape[1]
    high = sums.astype(BF16).astype(F32)
    row = lax.broadcasted_iota(jnp.int32, (8, rows), 0)
    packed = jnp.where(row == 0, high, jnp.where(row == 1, sums - high, 0.0))
    squares_ref[:, :rows] = packed.astype(BF16)
    squares_ref[:, rows:] = jnp.zeros((8, squares_ref.shape[1] - rows), BF16)


def first_up_body(
    h_hbm, gain_hbm, up_hbm, pieces_hbm, h_ref, gain_ref, up_ref, pieces_ref, small_sems, in_sems, out_sems
):
    chunks = in_sems.shape[0]
    width = up_ref.shape[1] // chunks
    per_chunk = pieces_ref.shape[0] // chunks
    small = [
        pltpu.make_async_copy(h_hbm, h_ref, small_sems.at[0]),
        pltpu.make_async_copy(gain_hbm, gain_ref, small_sems.at[1]),
    ]
    arriving = [
        pltpu.make_async_copy(
            up_hbm.at[:, pl.ds(i * width, width)], up_ref.at[:, pl.ds(i * width, width)], in_sems.at[i]
        )
        for i in range(chunks)
    ]
    leaving = [
        pltpu.make_async_copy(
            pieces_ref.at[pl.ds(i * per_chunk, per_chunk)],
            pieces_hbm.at[pl.ds(i * per_chunk, per_chunk)],
            out_sems.at[i],
        )
        for i in range(chunks)
    ]
    for copy in small + arriving:
        copy.start()
    if STAGGER_NS:

        @pl.when(lax.axis_index("dp") == STAGGER_CORE)
        def _():
            pl.delay(STAGGER_NS)

    for copy in small:
        copy.wait()
    scaled = (h_ref[...].astype(F32) * gain_ref[...]).astype(BF16)
    for i in range(chunks):
        arriving[i].wait()
        for piece in range(i * per_chunk, (i + 1) * per_chunk):
            write_pieces(scaled, up_ref, pieces_ref, piece)
        leaving[i].start()
    for copy in leaving:
        copy.wait()


def up_body(h_ref, gain_ref, up_ref, pieces_ref, squares_ref):
    h32 = h_ref[...].astype(F32)
    scaled = (h32 * gain_ref[:1]).astype(BF16)
    for piece in range(pieces_ref.shape[0]):
        write_pieces(scaled, up_ref, pieces_ref, piece)
    write_squares(h32, squares_ref)


def up_shapes(h, w_up):
    ra = lax.axis_size("ra")
    return (
        jax.ShapeDtypeStruct((ra, h.shape[0], w_up.shape[1] // ra), BF16),
        jax.ShapeDtypeStruct((8, h.shape[1]), BF16),
    )


def up_costs(h, w_up):
    return pl.CostEstimate(
        flops=2 * h.size * w_up.shape[1], bytes_accessed=UP_COST, transcendentals=0
    )


def first_up(h, gain, w_up):
    chunks = 4
    pieces, _ = up_shapes(h, w_up)
    hbm = pl.BlockSpec(memory_space=pl.ANY)
    return pl.pallas_call(
        first_up_body,
        out_shape=pieces,
        in_specs=[hbm] * 3,
        out_specs=hbm,
        scratch_shapes=[
            pltpu.VMEM(h.shape, h.dtype),
            pltpu.VMEM(gain.shape, gain.dtype),
            pltpu.VMEM(w_up.shape, w_up.dtype),
            pltpu.VMEM(pieces.shape, pieces.dtype),
            pltpu.SemaphoreType.DMA((2,)),
            pltpu.SemaphoreType.DMA((chunks,)),
            pltpu.SemaphoreType.DMA((chunks,)),
        ],
        compiler_params=pltpu.CompilerParams(vmem_limit_bytes=66_000_000),
        cost_estimate=up_costs(h, w_up),
        name="first_up",
    )(h, gain, w_up)


def second_up(h, gain, w_up):
    return pl.pallas_call(
        up_body,
        out_shape=up_shapes(h, w_up),
        compiler_params=pltpu.CompilerParams(vmem_limit_bytes=8 * 1024 * 1024),
        cost_estimate=up_costs(h, w_up),
        name="second_up",
    )(h, gain, w_up)


def branch_of(pieces, packed, w_down, beside):
    ra, rows, _ = pieces.shape
    arrived, packed, beside = lax.optimization_barrier((exchange(pieces, "ra"), packed, beside))
    shared = arrived.astype(F32).sum(axis=0)
    hidden_share = jnp.square(jax.nn.relu(shared)).astype(BF16)
    everyone = sent_to_all(jnp.concatenate([hidden_share, packed], axis=0), "ra")
    hidden = jnp.moveaxis(everyone[:, :rows], 0, 1).reshape(rows, -1)
    squares = everyone[:, rows : rows + 2, :rows].astype(F32).sum(axis=(0, 1))
    mean_sq = squares / (ra * packed.shape[1])
    down = jnp.dot(hidden, w_down, preferred_element_type=F32)
    return summed_over(down, "cb") / (mean_sq + EPS)[:, None], beside


def local(tokens, gain_first, up_first, down_first, gain_second, up_second, down_second, gain_last):
    pieces = first_up(tokens, gain_first[None, :], up_first)
    pieces, tokens, gain_second, gain_last = lax.optimization_barrier(
        (pieces, tokens, gain_second, gain_last)
    )
    start = tokens.astype(F32)
    gains = lax.optimization_barrier(
        tuple(jnp.broadcast_to(gain, (8, *gain.shape)) for gain in (gain_second, gain_last))
    )
    branch, gains = branch_of(pieces, packed_row(start), down_first, gains)
    first = (0.5 * start + branch).astype(BF16)
    pieces, packed = second_up(first, gains[0], up_second)
    branch, gains = branch_of(pieces, packed, down_second, gains)
    second = (0.5 * first.astype(F32) + branch).astype(BF16)
    second32 = second.astype(F32)
    squares = sent_to_all(jnp.sum(second32 * second32, axis=1), "ra").sum(axis=0)
    inverse = lax.rsqrt(squares / (lax.axis_size("ra") * second.shape[1]) + EPS)
    return (second32 * inverse[:, None] * gains[1][0]).astype(BF16)


def solution(mesh):
    return jax.shard_map(
        local,
        mesh=mesh,
        in_specs=(
            P(("grp", "dp"), "ra"),
            P("ra"),
            P("ra", "cb"),
            P("cb", "ra"),
            P("ra"),
            P("ra", "cb"),
            P("cb", "ra"),
            P("ra"),
        ),
        out_specs=P(("grp", "dp"), "ra"),
        check_vma=False,
    )
```

time: 162 us -> 143 us (0.88); the launches traced: 159 us -> 142 us
  Pallas kernels: 0 us -> 14.7 us
  blocking collectives: 71.3 us -> 59 us
  starting transfers between devices: 43.9 us -> 35.8 us
  waiting for transfers between devices: 35.1 us -> 29.5 us
  local copies, waits for them, and re-layouts: 5.27 us -> 1.37 us
    pallas_call x0 -> x2, Pallas kernels: none -> 14.7 us  [the longest x1 14.4 us: first_up(): pl.pallas_call(first_up_body, out_shape=pieces, in_specs=[hbm] * 3, out_s...]
    all_to_all x4 -> x2, starting transfers between devices: 43.9 us -> 29.8 us  [exchange(): return lax.all_to_all(pieces, axis, split_axis=0, concat_axis=0, tiled=True)]
    all_to_all x4 -> x2, waiting for transfers between devices: 35.1 us -> 22.7 us  [exchange(): return lax.all_to_all(pieces, axis, split_axis=0, concat_axis=0, tiled=True)]
    all_to_all x3, blocking collectives: 71.3 us -> 59 us  [exchange(): return lax.all_to_all(pieces, axis, split_axis=0, concat_axis=0, tiled=True)]
    ppermute x0 -> x6, waiting for transfers between devices: none -> 6.79 us  [summed_over(): lax.ppermute(value, axis, [(i, (i + step) % size) for i in range(size)])]
    ppermute x0 -> x6, starting transfers between devices: none -> 6.03 us  [summed_over(): lax.ppermute(value, axis, [(i, (i + step) % size) for i in range(size)])]
    unnamed x14 -> x12, local copies, waits for them, and re-layouts: 2.36 us -> 0.67 us
  transfers between devices with their start and end apart: 4 -> 8, of which waited for: 4 -> 7; matrix products, arithmetic and copies ran while one was open for 0% -> 0% of each run, Pallas kernels for 0% -> 0%
where the time goes in v2:
time: 143 us; the launch traced here: 142 us
  blocking collectives  59 us (41%)
  starting transfers between devices  35.8 us (25%)
  waiting for transfers between devices  29.5 us (21%)
  Pallas kernels  14.7 us (10%)
    all_to_all x3, blocking collectives, exchange(): return lax.all_to_all(pieces, axis, split_axis=0, concat_axis=0, tiled=True)  59 us
    all_to_all x2, starting transfers between devices, exchange(): return lax.all_to_all(pieces, axis, split_axis=0, concat_axis=0, tiled=True)  29.8 us
    all_to_all x2, waiting for transfers between devices, exchange(): return lax.all_to_all(pieces, axis, split_axis=0, concat_axis=0, tiled=True)  22.7 us
    pallas_call x1, Pallas kernels, first_up(): pl.pallas_call(first_up_body, out_shape=pieces, in_specs=[hbm] * 3, out_s...  14.4 us
    ppermute x6, waiting for transfers between devices, summed_over(): lax.ppermute(value, axis, [(i, (i + step) % size) for i in range(size)])  6.79 us
    ppermute x6, starting transfers between devices, summed_over(): lax.ppermute(value, axis, [(i, (i + step) % size) for i in range(size)])  6.03 us
  transfers between devices with their start and end apart: 8, of which 7 were waited for; matrix products, arithmetic and copies ran while one was open for 0% of the time, Pallas kernels for 0%

profile of v2, /device:TPU:33, one launch (start us, length us, event | category | flops | bytes accessed | tf_op | source)
XLA Modules:
  0.0 142.2 jit_solution(4531994389165812257)
XLA Ops:
  0.0 14.4 %first_up.1 = bf16[16,64,128]{2,1,0:T(8,128)(2,1)} custom-call(bf16[64,128]{1,0:T(8,128)(2,1)} %h_hbm.1, f32[1,128]{1,0:T(1,128)} %bitcast.26, bf16[128,2048]{1,0:T(8,128)(2,1)} %up_hbm.1), custom_call_target="tpu_custom_call" | custom-call | flops 33554432 | bytes 2097152 | tf_op jit(solution)/shard_map/first_up/pallas_call | solution.py:125
  14.4 24.5 %all-to-all-start = ((bf16[16,64,128]{2,1,0:T(8,128)(2,1)}), bf16[16,64,128]{2,1,0:T(8,128)(2,1)S(1)}, u32[]{:S(2)}, u32[]{:S(2)}) async-start(bf16[16,64,128]{2,1,0:T(8,128)(2,1)} %first_up.1), calls=%async_computation | async-start | bytes 524288 | tf_op jit(solution)/shard_map/all_to_all | solution.py:17
  39.0 0.6 copy-done.5
  39.8 11.7 %all-to-all-done = bf16[16,64,128]{2,1,0:T(8,128)(2,1)S(1)} async-done(((bf16[16,64,128]{2,1,0:T(8,128)(2,1)}), bf16[16,64,128]{2,1,0:T(8,128)(2,1)S(1)}, u32[]{:S(2)}, u32[]{:S(2)}) %all-to-all-start) | async-done | bytes 262176 | tf_op jit(solution)/shard_map/all_to_all | solution.py:17
  51.6 18.9 %all_to_all.26 = bf16[16,72,128]{2,1,0:T(8,128)(2,1)S(1)} all-to-all(bf16[16,72,128]{2,1,0:T(8,128)(2,1)S(1)} %broadcast_in_dim.24), channel_id=1, replica_groups=mesh['grp'=2,'ra'=16,'cb'=4,'dp'=2] {'ra'}, dimensions={0} | all-to-all | bytes 589824 | tf_op jit(solution)/shard_map/all_to_all | solution.py:17
  70.5 0.2 fusion.3
  70.8 3.0 %collective-permute-start.2 = (f32[64,128]{1,0:T(8,128)S(1)}, f32[64,128]{1,0:T(8,128)S(1)}, u32[]{:S(2)}, u32[]{:S(2)}) collective-permute-start(f32[64,128]{1,0:T(8,128)S(1)} %fusion.3), channel_id=1, source_target_pairs={{0,6},{2,0},{4,2},{6,4},{1,7},{3,1},{5,3},{7,5},{8,14},{10,8},{12,... | collective-permute-start | bytes 98312 | tf_op jit(solution)/shard_map/ppermute | solution.py:28
  73.8 0.3 collective-permute-start.1
  74.0 0.7 collective-permute-start
  74.8 3.3 %collective-permute-done.1 = f32[64,128]{1,0:T(8,128)S(1)} collective-permute-done((f32[64,128]{1,0:T(8,128)S(1)}, f32[64,128]{1,0:T(8,128)S(1)}, u32[]{:S(2)}, u32[]{:S(2)}) %collective-permute-start.1) | collective-permute-done | bytes 32800 | tf_op jit(solution)/shard_map/ppermute | solution.py:28
  78.1 0.2 collective-permute-done
  78.5 0.3 second_up.1
  78.7 18.7 %all_to_all.27 = bf16[16,64,128]{2,1,0:T(8,128)(2,1)S(1)} all-to-all(bf16[16,64,128]{2,1,0:T(8,128)(2,1)S(1)} %get-tuple-element.29), channel_id=1, replica_groups=mesh['grp'=2,'ra'=16,'cb'=4,'dp'=2] {'ra'}, dimensions={0} | all-to-all | bytes 524288 | tf_op jit(solution)/shard_map/all_to_all | solution.py:17
  97.6 21.3 %all_to_all.28 = bf16[16,72,128]{2,1,0:T(8,128)(2,1)S(1)} all-to-all(bf16[16,72,128]{2,1,0:T(8,128)(2,1)S(1)} %broadcast_in_dim.25), channel_id=1, replica_groups=mesh['grp'=2,'ra'=16,'cb'=4,'dp'=2] {'ra'}, dimensions={0} | all-to-all | bytes 589824 | tf_op jit(solution)/shard_map/all_to_all | solution.py:17
  119.2 0.4 collective-permute-start.5
  119.6 0.9 collective-permute-start.4
  120.5 0.7 collective-permute-start.3
  121.3 0.8 collective-permute-done.5
  122.1 1.8 %collective-permute-done.4 = f32[64,128]{1,0:T(8,128)S(1)} collective-permute-done((f32[64,128]{1,0:T(8,128)S(1)}, f32[64,128]{1,0:T(8,128)S(1)}, u32[]{:S(2)}, u32[]{:S(2)}) %collective-permute-start.4) | collective-permute-done | bytes 32800 | tf_op jit(solution)/shard_map/ppermute | solution.py:28
  123.8 0.6 collective-permute-done.3
  124.7 0.6 broadcast_in_dim.26
  125.3 5.2 %all-to-all-start.4 = ((f32[16,1,64]{2,1,0:T(1,128)}), f32[16,1,64]{2,1,0:T(1,128)S(1)}, u32[]{:S(2)}, u32[]{:S(2)}) async-start(f32[16,1,64]{2,1,0:T(1,128)} %broadcast_in_dim.26), calls=%async_computation.4 | async-start | bytes 16384 | tf_op jit(solution)/shard_map/all_to_all | solution.py:17
  130.5 11.0 %all-to-all-done.4 = f32[16,1,64]{2,1,0:T(1,128)S(1)} async-done(((f32[16,1,64]{2,1,0:T(1,128)}), f32[16,1,64]{2,1,0:T(1,128)S(1)}, u32[]{:S(2)}, u32[]{:S(2)}) %all-to-all-start.4) | async-done | bytes 4128 | tf_op jit(solution)/shard_map/all_to_all | solution.py:17
  141.5 0.7 fusion.11
  (35 shorter events, 1.0 us)
Async XLA Ops:
  0.0 70.5 %copy-start = (bf16[2048,128]{1,0:T(8,128)(2,1)S(1)}, bf16[2048,128]{1,0:T(8,128)(2,1)}, u32[]{:S(2)}) copy-start(bf16[2048,128]{1,0:T(8,128)(2,1)} %param.11) | copy-start | bytes 1572868
  14.4 24.6 %copy-start.4 = (f32[128]{0:T(128)S(1)}, f32[128]{0:T(128)}, u32[]{:S(2)}) copy-start(f32[128]{0:T(128)} %param.12) | copy-start | bytes 1540
  14.4 25.2 %copy-start.3 = (bf16[64,128]{1,0:T(8,128)(2,1)S(1)}, bf16[64,128]{1,0:T(8,128)(2,1)}, u32[]{:S(2)}) copy-start(bf16[64,128]{1,0:T(8,128)(2,1)} %h_hbm.1) | copy-start | bytes 49156
  14.4 37.1 %all-to-all-start = ((bf16[16,64,128]{2,1,0:T(8,128)(2,1)}), bf16[16,64,128]{2,1,0:T(8,128)(2,1)S(1)}, u32[]{:S(2)}, u32[]{:S(2)}) async-start(bf16[16,64,128]{2,1,0:T(8,128)(2,1)} %first_up.1), calls=%async_computation | async-start | bytes 524288 | tf_op jit(solution)/shard_map/all_to_all | solution.py:17
  39.0 0.7 copy-start.5
  70.5 7.9 %copy-start.1 = (bf16[128,2048]{1,0:T(8,128)(2,1)S(1)}, bf16[128,2048]{1,0:T(8,128)(2,1)}, u32[]{:S(2)}) copy-start(bf16[128,2048]{1,0:T(8,128)(2,1)} %up_ref.1) | copy-start | bytes 1572868
  70.8 4.0 %collective-permute-start.2 = (f32[64,128]{1,0:T(8,128)S(1)}, f32[64,128]{1,0:T(8,128)S(1)}, u32[]{:S(2)}, u32[]{:S(2)}) collective-permute-start(f32[64,128]{1,0:T(8,128)S(1)} %fusion.3), channel_id=1, source_target_pairs={{0,6},{2,0},{4,2},{6,4},{1,7},{3,1},{5,3},{7,5},{8,14},{10,8},{12,... | collective-permute-start | bytes 98312 | tf_op jit(solution)/shard_map/ppermute | solution.py:28
  73.8 4.4 %collective-permute-start.1 = (f32[64,128]{1,0:T(8,128)S(1)}, f32[64,128]{1,0:T(8,128)S(1)}, u32[]{:S(2)}, u32[]{:S(2)}) collective-permute-start(f32[64,128]{1,0:T(8,128)S(1)} %fusion.3), channel_id=1, source_target_pairs={{0,4},{2,6},{4,0},{6,2},{1,5},{3,7},{5,1},{7,3},{8,12},{10,14},{12... | collective-permute-start | bytes 98312 | tf_op jit(solution)/shard_map/ppermute | solution.py:28
  74.0 4.3 %collective-permute-start = (f32[64,128]{1,0:T(8,128)S(1)}, f32[64,128]{1,0:T(8,128)S(1)}, u32[]{:S(2)}, u32[]{:S(2)}) collective-permute-start(f32[64,128]{1,0:T(8,128)S(1)} %fusion.3), channel_id=1, source_target_pairs={{0,2},{2,4},{4,6},{6,0},{1,3},{3,5},{5,7},{7,1},{8,10},{10,12},{12... | collective-permute-start | bytes 98312 | tf_op jit(solution)/shard_map/ppermute | solution.py:28
  97.5 21.4 %copy-start.2 = (bf16[2048,128]{1,0:T(8,128)(2,1)S(1)}, bf16[2048,128]{1,0:T(8,128)(2,1)}, u32[]{:S(2)}) copy-start(bf16[2048,128]{1,0:T(8,128)(2,1)} %param.14) | copy-start | bytes 1572868
  119.2 2.9 %collective-permute-start.5 = (f32[64,128]{1,0:T(8,128)S(1)}, f32[64,128]{1,0:T(8,128)S(1)}, u32[]{:S(2)}, u32[]{:S(2)}) collective-permute-start(f32[64,128]{1,0:T(8,128)S(1)} %fusion), channel_id=1, source_target_pairs={{0,6},{2,0},{4,2},{6,4},{1,7},{3,1},{5,3},{7,5},{8,14},{10,8},{12,... | collective-permute-start | bytes 98312 | tf_op jit(solution)/shard_map/ppermute | solution.py:28
  119.6 4.3 %collective-permute-start.4 = (f32[64,128]{1,0:T(8,128)S(1)}, f32[64,128]{1,0:T(8,128)S(1)}, u32[]{:S(2)}, u32[]{:S(2)}) collective-permute-start(f32[64,128]{1,0:T(8,128)S(1)} %fusion), channel_id=1, source_target_pairs={{0,4},{2,6},{4,0},{6,2},{1,5},{3,7},{5,1},{7,3},{8,12},{10,14},{12... | collective-permute-start | bytes 98312 | tf_op jit(solution)/shard_map/ppermute | solution.py:28
  120.5 4.0 %collective-permute-start.3 = (f32[64,128]{1,0:T(8,128)S(1)}, f32[64,128]{1,0:T(8,128)S(1)}, u32[]{:S(2)}, u32[]{:S(2)}) collective-permute-start(f32[64,128]{1,0:T(8,128)S(1)} %fusion), channel_id=1, source_target_pairs={{0,2},{2,4},{4,6},{6,0},{1,3},{3,5},{5,7},{7,1},{8,10},{10,12},{12... | collective-permute-start | bytes 98312 | tf_op jit(solution)/shard_map/ppermute | solution.py:28
  125.3 16.2 %all-to-all-start.4 = ((f32[16,1,64]{2,1,0:T(1,128)}), f32[16,1,64]{2,1,0:T(1,128)S(1)}, u32[]{:S(2)}, u32[]{:S(2)}) async-start(f32[16,1,64]{2,1,0:T(1,128)} %broadcast_in_dim.26), calls=%async_computation.4 | async-start | bytes 16384 | tf_op jit(solution)/shard_map/all_to_all | solution.py:17

commit v3 on v2

--- a/solution.py
+++ b/solution.py
@@ -10,22 +10,34 @@
 BF16 = jnp.bfloat16
 STAGGER_NS = 13000
 STAGGER_CORE = 1
+LEAD_EIGHTHS = 6
+SUM_TYPE = BF16
 UP_COST = 2 << 20
 
 
-def exchange(pieces, axis):
-    return lax.all_to_all(pieces, axis, split_axis=0, concat_axis=0, tiled=True)
-
-
-def sent_to_all(shard, axis):
-    return exchange(jnp.broadcast_to(shard, (lax.axis_size(axis), *shard.shape)), axis)
+def turned(size):
+    lead = size * LEAD_EIGHTHS // 8
+    return [(lead + i) % size for i in range(size)]
+
+
+def exchange(pieces):
+    order = turned(lax.axis_size("ra"))
+    return lax.all_to_all(
+        pieces, "ra", split_axis=0, concat_axis=0, tiled=True, axis_index_groups=[order]
+    )
+
+
+def sent_to_all(shard):
+    return exchange(jnp.broadcast_to(shard, (lax.axis_size("ra"), *shard.shape)))
 
 
 def summed_over(value, axis):
     size = lax.axis_size(axis)
     total = value
+    sent = value.astype(SUM_TYPE)
     for step in range(1, size):
-        total = total + lax.ppermute(value, axis, [(i, (i + step) % size) for i in range(size)])
+        pairs = [(i, (i + step) % size) for i in range(size)]
+        total = total + lax.ppermute(sent, axis, pairs).astype(F32)
     return total
 
 
@@ -39,7 +51,7 @@
 def write_pieces(scaled, up_ref, pieces_ref, piece):
     width = pieces_ref.shape[2]
     lanes = pl.ds(piece * width, width)
-    pieces_ref[piece] = jnp.dot(scaled, up_ref[:, lanes], preferred_element_type=F32).astype(BF16)
+    pieces_ref[turned(pieces_ref.shape[0]).index(piece)] = jnp.dot(scaled, up_ref[:, lanes], preferred_element_type=F32).astype(BF16)
 
 
 def write_squares(h32, squares_ref):
@@ -58,6 +70,7 @@
     chunks = in_sems.shape[0]
     width = up_ref.shape[1] // chunks
     per_chunk = pieces_ref.shape[0] // chunks
+    order = turned(pieces_ref.shape[0])
     small = [
         pltpu.make_async_copy(h_hbm, h_ref, small_sems.at[0]),
         pltpu.make_async_copy(gain_hbm, gain_ref, small_sems.at[1]),
@@ -91,7 +104,7 @@
         arriving[i].wait()
         for piece in range(i * per_chunk, (i + 1) * per_chunk):
             write_pieces(scaled, up_ref, pieces_ref, piece)
-        leaving[i].start()
+        leaving[order.index(i * per_chunk) // per_chunk].start()
     for copy in leaving:
         copy.wait()
 
@@ -152,16 +165,40 @@
     )(h, gain, w_up)
 
 
+def down_body(everyone_ref, down_ref, out_ref):
+    rows, lanes = out_ref.shape[0], everyone_ref.shape[2]
+    order = turned(everyone_ref.shape[0])
+    total = jnp.zeros(out_ref.shape, F32)
+    for block in range(0, len(order), 2):
+        pair = [everyone_ref[order.index(block + k), :rows, :] for k in range(2)]
+        weights = down_ref[pl.ds(block * lanes, 2 * lanes), :]
+        total = total + jnp.dot(
+            jnp.concatenate(pair, axis=1), weights, preferred_element_type=F32
+        )
+    out_ref[...] = total
+
+
+def down_sums(everyone, w_down, rows):
+    return pl.pallas_call(
+        down_body,
+        out_shape=jax.ShapeDtypeStruct((rows, w_down.shape[1]), F32),
+        compiler_params=pltpu.CompilerParams(vmem_limit_bytes=8 * 1024 * 1024),
+        cost_estimate=pl.CostEstimate(
+            flops=2 * rows * w_down.size, bytes_accessed=UP_COST, transcendentals=0
+        ),
+        name="down_sums",
+    )(everyone, w_down)
+
+
 def branch_of(pieces, packed, w_down, beside):
     ra, rows, _ = pieces.shape
-    arrived, packed, beside = lax.optimization_barrier((exchange(pieces, "ra"), packed, beside))
+    arrived, packed, beside = lax.optimization_barrier((exchange(pieces), packed, beside))
     shared = arrived.astype(F32).sum(axis=0)
     hidden_share = jnp.square(jax.nn.relu(shared)).astype(BF16)
-    everyone = sent_to_all(jnp.concatenate([hidden_share, packed], axis=0), "ra")
-    hidden = jnp.moveaxis(everyone[:, :rows], 0, 1).reshape(rows, -1)
+    everyone = sent_to_all(jnp.concatenate([hidden_share, packed], axis=0))
     squares = everyone[:, rows : rows + 2, :rows].astype(F32).sum(axis=(0, 1))
     mean_sq = squares / (ra * packed.shape[1])
-    down = jnp.dot(hidden, w_down, preferred_element_type=F32)
+    down = down_sums(everyone, w_down, rows)
     return summed_over(down, "cb") / (mean_sq + EPS)[:, None], beside
 
 
@@ -172,7 +209,7 @@
     )
     start = tokens.astype(F32)
     gains = lax.optimization_barrier(
-        tuple(jnp.broadcast_to(gain, (8, *gain.shape)) for gain in (gain_second, gain_last))
+        tuple(jnp.broadcast_to(gain, (*tokens.shape[:1], *gain.shape)) for gain in (gain_second, gain_last))
     )
     branch, gains = branch_of(pieces, packed_row(start), down_first, gains)
     first = (0.5 * start + branch).astype(BF16)
@@ -180,9 +217,9 @@
     branch, gains = branch_of(pieces, packed, down_second, gains)
     second = (0.5 * first.astype(F32) + branch).astype(BF16)
     second32 = second.astype(F32)
-    squares = sent_to_all(jnp.sum(second32 * second32, axis=1), "ra").sum(axis=0)
+    squares = sent_to_all(jnp.sum(second32 * second32, axis=1)).sum(axis=0)
     inverse = lax.rsqrt(squares / (lax.axis_size("ra") * second.shape[1]) + EPS)
-    return (second32 * inverse[:, None] * gains[1][0]).astype(BF16)
+    return (second32 * inverse[:, None] * gains[1]).astype(BF16)
 
 
 def solution(mesh):

time: 143 us -> 140 us (0.979)
  waiting for transfers between devices: 29.5 us -> 15.6 us
  blocking collectives: 59 us -> 71.9 us
  starting transfers between devices: 35.8 us -> 33.7 us
    all_to_all x2 -> x1, waiting for transfers between devices: 22.7 us -> 9.29 us  [exchange(): lax.all_to_all(pieces, 'ra', split_axis=0, concat_axis=0, tiled=True, axi...]
    all_to_all x3 -> x4, blocking collectives: 59 us -> 71.9 us  [exchange(): lax.all_to_all(pieces, 'ra', split_axis=0, concat_axis=0, tiled=True, axi...]
    all_to_all x2 -> x1, starting transfers between devices: 29.8 us -> 27.2 us  [exchange(): lax.all_to_all(pieces, 'ra', split_axis=0, concat_axis=0, tiled=True, axi...]
  transfers between devices with their start and end apart: 8 -> 7, of which waited for: 7 -> 6; matrix products, arithmetic and copies ran while one was open for 0% -> 0% of each run, Pallas kernels for 0% -> 0%
where the time goes in v3:
time: 140 us; the launch traced here: 139 us
  blocking collectives  71.9 us (51%)
  starting transfers between devices  33.7 us (24%)
  waiting for transfers between devices  15.6 us (11%)
  Pallas kernels  15.1 us (11%)
  local copies, waits for them, and re-layouts  1.47 us (1%)
    all_to_all x4, blocking collectives, exchange(): lax.all_to_all(pieces, 'ra', split_axis=0, concat_axis=0, tiled=True, axi...  71.9 us
    all_to_all x1, starting transfers between devices, exchange(): lax.all_to_all(pieces, 'ra', split_axis=0, concat_axis=0, tiled=True, axi...  27.2 us
    pallas_call x1, Pallas kernels, first_up(): pl.pallas_call(first_up_body, out_shape=pieces, in_specs=[hbm] * 3, out_s...  14.4 us
    all_to_all x1, waiting for transfers between devices, exchange(): lax.all_to_all(pieces, 'ra', split_axis=0, concat_axis=0, tiled=True, axi...  9.29 us
    ppermute x6, starting transfers between devices, summed_over(): total = total + lax.ppermute(sent, axis, pairs).astype(F32)  6.53 us
    ppermute x6, waiting for transfers between devices, summed_over(): total = total + lax.ppermute(sent, axis, pairs).astype(F32)  6.26 us
  transfers between devices with their start and end apart: 7, of which 6 were waited for; matrix products, arithmetic and copies ran while one was open for 0% of the time, Pallas kernels for 0%

profile of v3, /device:TPU:33, one launch (start us, length us, event | category | flops | bytes accessed | tf_op | source)
XLA Modules:
  0.0 139.3 jit_solution(10667782618768873396)
XLA Ops:
  0.0 14.4 %first_up.1 = bf16[16,64,128]{2,1,0:T(8,128)(2,1)} custom-call(bf16[64,128]{1,0:T(8,128)(2,1)} %h_hbm.1, f32[1,128]{1,0:T(1,128)} %bitcast.6, bf16[128,2048]{1,0:T(8,128)(2,1)} %up_hbm.1), custom_call_target="tpu_custom_call" | custom-call | flops 33554432 | bytes 2097152 | tf_op jit(solution)/shard_map/first_up/pallas_call | solution.py:138
  14.4 27.2 %all-to-all-start = ((bf16[16,64,128]{2,1,0:T(8,128)(2,1)}), bf16[16,64,128]{2,1,0:T(8,128)(2,1)S(1)}, u32[]{:S(2)}, u32[]{:S(2)}) async-start(bf16[16,64,128]{2,1,0:T(8,128)(2,1)} %first_up.1), calls=%async_computation | async-start | bytes 524288 | tf_op jit(solution)/shard_map/all_to_all | solution.py:25
  41.7 0.6 copy-done.5
  42.3 0.7 copy-done.3
  43.1 9.3 %all-to-all-done = bf16[16,64,128]{2,1,0:T(8,128)(2,1)S(1)} async-done(((bf16[16,64,128]{2,1,0:T(8,128)(2,1)}), bf16[16,64,128]{2,1,0:T(8,128)(2,1)S(1)}, u32[]{:S(2)}, u32[]{:S(2)}) %all-to-all-start) | async-done | bytes 262176 | tf_op jit(solution)/shard_map/all_to_all | solution.py:25
  52.6 19.3 %all_to_all.26.everyone_ref = bf16[16,72,128]{2,1,0:T(8,128)(2,1)S(1)} all-to-all(bf16[16,72,128]{2,1,0:T(8,128)(2,1)S(1)} %broadcast_in_dim.24), channel_id=1, replica_groups={{96,104,112,120,0,8,16,24,32,40,48,56,64,72,80,88},{97,105,113,121,1,9,..., dimensions={0} | all-to-all | bytes 589824 | tf_op jit(solution)/shard_map/all_to_all | solution.py:25
  71.9 0.2 down_sums.2
  72.1 3.0 %collective-permute-start.2 = (bf16[64,128]{1,0:T(8,128)(2,1)S(1)}, bf16[64,128]{1,0:T(8,128)(2,1)S(1)}, u32[]{:S(2)}, u32[]{:S(2)}) collective-permute-start(bf16[64,128]{1,0:T(8,128)(2,1)S(1)} %convert_element_type.66), channel_id=1, source_target_pairs={{0,6},{2,0},{4,2},{6,4},{1,7},{3,1},{5,3},{7,5},{8,14},{10,8},{12,... | collective-permute-start | bytes 49160 | tf_op jit(solution)/shard_map/ppermute | solution.py:40
  75.1 0.3 collective-permute-start.1
  75.4 0.7 collective-permute-start
  76.2 3.2 %collective-permute-done.1 = bf16[64,128]{1,0:T(8,128)(2,1)S(1)} collective-permute-done((bf16[64,128]{1,0:T(8,128)(2,1)S(1)}, bf16[64,128]{1,0:T(8,128)(2,1)S(1)}, u32[]{:S(2)}, u32[]{:S(2)}) %collective-permute-start.1) | collective-permute-done | bytes 16416 | tf_op jit(solution)/shard_map/ppermute | solution.py:40
  79.5 0.3 second_up.1
  79.7 18.5 %all_to_all.27 = bf16[16,64,128]{2,1,0:T(8,128)(2,1)S(1)} all-to-all(bf16[16,64,128]{2,1,0:T(8,128)(2,1)S(1)} %get-tuple-element.29), channel_id=1, replica_groups={{96,104,112,120,0,8,16,24,32,40,48,56,64,72,80,88},{97,105,113,121,1,9,..., dimensions={0} | all-to-all | bytes 524288 | tf_op jit(solution)/shard_map/all_to_all | solution.py:25
  98.4 20.1 %all_to_all.28.everyone_ref = bf16[16,72,128]{2,1,0:T(8,128)(2,1)S(1)} all-to-all(bf16[16,72,128]{2,1,0:T(8,128)(2,1)S(1)} %broadcast_in_dim.25), channel_id=1, replica_groups={{96,104,112,120,0,8,16,24,32,40,48,56,64,72,80,88},{97,105,113,121,1,9,..., dimensions={0} | all-to-all | bytes 589824 | tf_op jit(solution)/shard_map/all_to_all | solution.py:25
  118.5 0.2 down_sums.3
  118.8 0.3 collective-permute-start.5
  119.1 1.5 %collective-permute-start.4 = (bf16[64,128]{1,0:T(8,128)(2,1)S(1)}, bf16[64,128]{1,0:T(8,128)(2,1)S(1)}, u32[]{:S(2)}, u32[]{:S(2)}) collective-permute-start(bf16[64,128]{1,0:T(8,128)(2,1)S(1)} %convert_element_type.75), channel_id=1, source_target_pairs={{0,4},{2,6},{4,0},{6,2},{1,5},{3,7},{5,1},{7,3},{8,12},{10,14},{12... | collective-permute-start | bytes 49160 | tf_op jit(solution)/shard_map/ppermute | solution.py:40
  120.6 0.7 collective-permute-start.3
  121.4 0.1 collective-permute-done.5
  121.5 1.7 %collective-permute-done.4 = bf16[64,128]{1,0:T(8,128)(2,1)S(1)} collective-permute-done((bf16[64,128]{1,0:T(8,128)(2,1)S(1)}, bf16[64,128]{1,0:T(8,128)(2,1)S(1)}, u32[]{:S(2)}, u32[]{:S(2)}) %collective-permute-start.4) | collective-permute-done | bytes 16416 | tf_op jit(solution)/shard_map/ppermute | solution.py:40
  123.2 1.2 collective-permute-done.3
  124.4 0.2 fusion.3
  124.6 14.0 %all_to_all.29 = f32[16,1,64]{2,1,0:T(1,128)S(1)} all-to-all(f32[16,1,64]{2,1,0:T(1,128)S(1)} %broadcast_in_dim.26), channel_id=1, replica_groups={{96,104,112,120,0,8,16,24,32,40,48,56,64,72,80,88},{97,105,113,121,1,9,..., dimensions={0} | all-to-all | bytes 8192 | tf_op jit(solution)/shard_map/all_to_all | solution.py:25
  138.6 0.7 fusion.5
  (35 shorter events, 0.6 us)
Async XLA Ops:
  14.4 27.2 %copy-start.4 = (f32[128]{0:T(128)S(1)}, f32[128]{0:T(128)}, u32[]{:S(2)}) copy-start(f32[128]{0:T(128)} %param.12) | copy-start | bytes 1540
  14.4 38.0 %all-to-all-start = ((bf16[16,64,128]{2,1,0:T(8,128)(2,1)}), bf16[16,64,128]{2,1,0:T(8,128)(2,1)S(1)}, u32[]{:S(2)}, u32[]{:S(2)}) async-start(bf16[16,64,128]{2,1,0:T(8,128)(2,1)} %first_up.1), calls=%async_computation | async-start | bytes 524288 | tf_op jit(solution)/shard_map/all_to_all | solution.py:25
  41.6 0.7 copy-start.5
  42.3 0.7 copy-start.3
  52.5 19.4 %copy-start.1 = (bf16[2048,128]{1,0:T(8,128)(2,1)S(1)}, bf16[2048,128]{1,0:T(8,128)(2,1)}, u32[]{:S(2)}) copy-start(bf16[2048,128]{1,0:T(8,128)(2,1)} %down_ref.2) | copy-start | bytes 1572868
  71.9 7.6 %copy-start = (bf16[128,2048]{1,0:T(8,128)(2,1)S(1)}, bf16[128,2048]{1,0:T(8,128)(2,1)}, u32[]{:S(2)}) copy-start(bf16[128,2048]{1,0:T(8,128)(2,1)} %up_ref.1) | copy-start | bytes 1572868
  72.1 4.0 %collective-permute-start.2 = (bf16[64,128]{1,0:T(8,128)(2,1)S(1)}, bf16[64,128]{1,0:T(8,128)(2,1)S(1)}, u32[]{:S(2)}, u32[]{:S(2)}) collective-permute-start(bf16[64,128]{1,0:T(8,128)(2,1)S(1)} %convert_element_type.66), channel_id=1, source_target_pairs={{0,6},{2,0},{4,2},{6,4},{1,7},{3,1},{5,3},{7,5},{8,14},{10,8},{12,... | collective-permute-start | bytes 49160 | tf_op jit(solution)/shard_map/ppermute | solution.py:40
  75.1 4.2 %collective-permute-start.1 = (bf16[64,128]{1,0:T(8,128)(2,1)S(1)}, bf16[64,128]{1,0:T(8,128)(2,1)S(1)}, u32[]{:S(2)}, u32[]{:S(2)}) collective-permute-start(bf16[64,128]{1,0:T(8,128)(2,1)S(1)} %convert_element_type.66), channel_id=1, source_target_pairs={{0,4},{2,6},{4,0},{6,2},{1,5},{3,7},{5,1},{7,3},{8,12},{10,14},{12... | collective-permute-start | bytes 49160 | tf_op jit(solution)/shard_map/ppermute | solution.py:40
  75.4 4.0 %collective-permute-start = (bf16[64,128]{1,0:T(8,128)(2,1)S(1)}, bf16[64,128]{1,0:T(8,128)(2,1)S(1)}, u32[]{:S(2)}, u32[]{:S(2)}) collective-permute-start(bf16[64,128]{1,0:T(8,128)(2,1)S(1)} %convert_element_type.66), channel_id=1, source_target_pairs={{0,2},{2,4},{4,6},{6,0},{1,3},{3,5},{5,7},{7,1},{8,10},{10,12},{12... | collective-permute-start | bytes 49160 | tf_op jit(solution)/shard_map/ppermute | solution.py:40
  98.3 20.2 %copy-start.2 = (bf16[2048,128]{1,0:T(8,128)(2,1)S(1)}, bf16[2048,128]{1,0:T(8,128)(2,1)}, u32[]{:S(2)}) copy-start(bf16[2048,128]{1,0:T(8,128)(2,1)} %down_ref.3) | copy-start | bytes 1572868
  118.8 2.7 %collective-permute-start.5 = (bf16[64,128]{1,0:T(8,128)(2,1)S(1)}, bf16[64,128]{1,0:T(8,128)(2,1)S(1)}, u32[]{:S(2)}, u32[]{:S(2)}) collective-permute-start(bf16[64,128]{1,0:T(8,128)(2,1)S(1)} %convert_element_type.75), channel_id=1, source_target_pairs={{0,6},{2,0},{4,2},{6,4},{1,7},{3,1},{5,3},{7,5},{8,14},{10,8},{12,... | collective-permute-start | bytes 49160 | tf_op jit(solution)/shard_map/ppermute | solution.py:40
  119.1 4.1 %collective-permute-start.4 = (bf16[64,128]{1,0:T(8,128)(2,1)S(1)}, bf16[64,128]{1,0:T(8,128)(2,1)S(1)}, u32[]{:S(2)}, u32[]{:S(2)}) collective-permute-start(bf16[64,128]{1,0:T(8,128)(2,1)S(1)} %convert_element_type.75), channel_id=1, source_target_pairs={{0,4},{2,6},{4,0},{6,2},{1,5},{3,7},{5,1},{7,3},{8,12},{10,14},{12... | collective-permute-start | bytes 49160 | tf_op jit(solution)/shard_map/ppermute | solution.py:40
  120.6 3.8 %collective-permute-start.3 = (bf16[64,128]{1,0:T(8,128)(2,1)S(1)}, bf16[64,128]{1,0:T(8,128)(2,1)S(1)}, u32[]{:S(2)}, u32[]{:S(2)}) collective-permute-start(bf16[64,128]{1,0:T(8,128)(2,1)S(1)} %convert_element_type.75), channel_id=1, source_target_pairs={{0,2},{2,4},{4,6},{6,0},{1,3},{3,5},{5,7},{7,1},{8,10},{10,12},{12... | collective-permute-start | bytes 49160 | tf_op jit(solution)/shard_map/ppermute | solution.py:40

commit v4 on v3

v4 whole, which is shorter than its diff:
```python
import jax
import jax.numpy as jnp
from jax import lax
from jax.experimental import pallas as pl
from jax.experimental.pallas import tpu as pltpu
from jax.sharding import PartitionSpec as P

EPS = 1e-06
F32 = jnp.float32
BF16 = jnp.bfloat16
STAGGER_NS = 12800
STAGGER_CORE = 1
LEAD_EIGHTHS = 7
LAST_LEAD_EIGHTHS = 4
SUM_TYPE = BF16
UP_COST = 2 << 20
PAD = 8
CHUNKS = 2


def member_order(size, eighths=None):
    lead = size * (LEAD_EIGHTHS if eighths is None else eighths) // 8
    return [(lead + i) % size for i in range(size)]


def exchange(pieces, eighths=None):
    order = member_order(lax.axis_size("ra"), eighths)
    return lax.all_to_all(
        pieces, "ra", split_axis=0, concat_axis=0, tiled=True, axis_index_groups=[order]
    )


def sent_to_all(shard, eighths=None):
    return exchange(jnp.broadcast_to(shard, (lax.axis_size("ra"), *shard.shape)), eighths)


def summed_over(value, axis):
    size = lax.axis_size(axis)
    total = value
    sent = value.astype(SUM_TYPE)
    for step in range(1, size):
        pairs = [(i, (i + step) % size) for i in range(size)]
        total = total + lax.ppermute(sent, axis, pairs).astype(F32)
    return total


def write_piece(scaled, packed, up_ref, pieces_ref, piece):
    width = pieces_ref.shape[2]
    lanes = pl.ds(piece * width, width)
    sums = jnp.dot(scaled, up_ref[:, lanes], preferred_element_type=F32)
    place = member_order(pieces_ref.shape[0]).index(piece)
    pieces_ref[place, : scaled.shape[0], :] = sums.astype(BF16)
    pieces_ref[place, scaled.shape[0] :, :] = packed


def squares_row(h32):
    lanes = h32.shape[1]
    square = h32 * h32
    sums = jnp.sum(jnp.transpose(square), axis=0, keepdims=True)
    high = sums.astype(BF16).astype(F32)
    row = lax.broadcasted_iota(jnp.int32, (PAD, sums.shape[1]), 0)
    packed = jnp.where(row == 0, high, jnp.where(row == 1, sums - high, 0.0))
    rest = jnp.zeros((PAD, lanes - sums.shape[1]), F32)
    return jnp.concatenate([packed, rest], axis=1).astype(BF16)


def first_up_body(
    h_hbm, gain_hbm, up_hbm, pieces_hbm, h_ref, gain_ref, up_ref, pieces_ref, small_sems, in_sems, out_sems
):
    chunks = in_sems.shape[0]
    width = up_ref.shape[1] // chunks
    per_chunk = pieces_ref.shape[0] // chunks
    order = member_order(pieces_ref.shape[0])
    small = [
        pltpu.make_async_copy(h_hbm, h_ref, small_sems.at[0]),
        pltpu.make_async_copy(gain_hbm, gain_ref, small_sems.at[1]),
    ]
    arriving = [
        pltpu.make_async_copy(
            up_hbm.at[:, pl.ds(i * width, width)], up_ref.at[:, pl.ds(i * width, width)], in_sems.at[i]
        )
        for i in range(chunks)
    ]
    leaving = [
        pltpu.make_async_copy(
            pieces_ref.at[order.index(piece)], pieces_hbm.at[order.index(piece)], out_sems.at[piece]
        )
        for piece in range(len(order))
    ]
    for copy in small + arriving:
        copy.start()
    if STAGGER_NS:

        @pl.when(lax.axis_index("dp") == STAGGER_CORE)
        def _():
            pl.delay(STAGGER_NS)

    for copy in small:
        copy.wait()
    h32 = h_ref[...].astype(F32)
    scaled = (h32 * gain_ref[...]).astype(BF16)
    packed = squares_row(h32)
    for i in range(chunks):
        arriving[i].wait()
        for piece in range(i * per_chunk, (i + 1) * per_chunk):
            write_piece(scaled, packed, up_ref, pieces_ref, piece)
            leaving[piece].start()
    for copy in leaving:
        copy.wait()


def up_body(h_ref, gain_ref, up_ref, pieces_ref):
    h32 = h_ref[...].astype(F32)
    scaled = (h32 * gain_ref[:1]).astype(BF16)
    packed = squares_row(h32)
    for piece in range(pieces_ref.shape[0]):
        write_piece(scaled, packed, up_ref, pieces_ref, piece)


def up_shape(h, w_up):
    ra = lax.axis_size("ra")
    return jax.ShapeDtypeStruct((ra, h.shape[0] + PAD, w_up.shape[1] // ra), BF16)


def up_costs(h, w_up):
    return pl.CostEstimate(
        flops=2 * h.size * w_up.shape[1], bytes_accessed=UP_COST, transcendentals=0
    )


def first_up(h, gain, w_up):
    chunks = CHUNKS
    pieces = up_shape(h, w_up)
    hbm = pl.BlockSpec(memory_space=pl.ANY)
    return pl.pallas_call(
        first_up_body,
        out_shape=pieces,
        in_specs=[hbm] * 3,
        out_specs=hbm,
        scratch_shapes=[
            pltpu.VMEM(h.shape, h.dtype),
            pltpu.VMEM(gain.shape, gain.dtype),
            pltpu.VMEM(w_up.shape, w_up.dtype),
            pltpu.VMEM(pieces.shape, pieces.dtype),
            pltpu.SemaphoreType.DMA((2,)),
            pltpu.SemaphoreType.DMA((chunks,)),
            pltpu.SemaphoreType.DMA(pieces.shape[:1]),
        ],
        compiler_params=pltpu.CompilerParams(vmem_limit_bytes=66_000_000),
        cost_estimate=up_costs(h, w_up),
        name="first_up",
    )(h, gain, w_up)


def second_up(h, gain, w_up):
    return pl.pallas_call(
        up_body,
        out_shape=up_shape(h, w_up),
        compiler_params=pltpu.CompilerParams(vmem_limit_bytes=8 * 1024 * 1024),
        cost_estimate=up_costs(h, w_up),
        name="second_up",
    )(h, gain, w_up)


def down_body(everyone_ref, down_ref, out_ref):
    rows, lanes = out_ref.shape[0], everyone_ref.shape[2]
    order = member_order(everyone_ref.shape[0])
    total = jnp.zeros(out_ref.shape, F32)
    for block in range(0, len(order), 2):
        pair = [everyone_ref[order.index(block + k), :rows, :] for k in range(2)]
        weights = down_ref[pl.ds(block * lanes, 2 * lanes), :]
        total = total + jnp.dot(
            jnp.concatenate(pair, axis=1), weights, preferred_element_type=F32
        )
    out_ref[...] = total


def down_sums(everyone, w_down, rows):
    return pl.pallas_call(
        down_body,
        out_shape=jax.ShapeDtypeStruct((rows, w_down.shape[1]), F32),
        compiler_params=pltpu.CompilerParams(vmem_limit_bytes=8 * 1024 * 1024),
        cost_estimate=pl.CostEstimate(
            flops=2 * rows * w_down.size, bytes_accessed=UP_COST, transcendentals=0
        ),
        name="down_sums",
    )(everyone, w_down)


def branch_of(pieces, w_down, beside):
    ra, rows, lanes = pieces.shape
    rows -= PAD
    arrived, beside = lax.optimization_barrier((exchange(pieces), beside))
    shared = arrived[:, :rows].astype(F32).sum(axis=0)
    hidden_share = jnp.square(jax.nn.relu(shared)).astype(BF16)
    squares = arrived[:, rows : rows + 2, :rows].astype(F32).sum(axis=(0, 1))
    hidden_share, squares = lax.optimization_barrier((hidden_share, squares))
    everyone = sent_to_all(hidden_share)
    mean_sq = squares / (ra * w_down.shape[1])
    down = down_sums(everyone, w_down, rows)
    return summed_over(down, "cb") / (mean_sq + EPS)[:, None], beside


def local(tokens, gain_first, up_first, down_first, gain_second, up_second, down_second, gain_last):
    pieces = first_up(tokens, gain_first[None, :], up_first)
    pieces, tokens, gain_second, gain_last = lax.optimization_barrier(
        (pieces, tokens, gain_second, gain_last)
    )
    start = tokens.astype(F32)
    gains = lax.optimization_barrier(
        tuple(jnp.broadcast_to(gain, (*tokens.shape[:1], *gain.shape)) for gain in (gain_second, gain_last))
    )
    branch, gains = branch_of(pieces, down_first, gains)
    first = (0.5 * start + branch).astype(BF16)
    pieces = second_up(first, gains[0], up_second)
    branch, gains = branch_of(pieces, down_second, gains)
    second = (0.5 * first.astype(F32) + branch).astype(BF16)
    second32 = second.astype(F32)
    squares = sent_to_all(jnp.sum(second32 * second32, axis=1), LAST_LEAD_EIGHTHS).sum(axis=0)
    inverse = lax.rsqrt(squares / (lax.axis_size("ra") * second.shape[1]) + EPS)
    return (second32 * inverse[:, None] * gains[1]).astype(BF16)


def solution(mesh):
    return jax.shard_map(
        local,
        mesh=mesh,
        in_specs=(
            P(("grp", "dp"), "ra"),
            P("ra"),
            P("ra", "cb"),
            P("cb", "ra"),
            P("ra"),
            P("ra", "cb"),
            P("cb", "ra"),
            P("ra"),
        ),
        out_specs=P(("grp", "dp"), "ra"),
        check_vma=False,
    )
```

time: 140 us -> 138 us (0.986)
  waiting for transfers between devices: 15.6 us -> 17.5 us
  starting transfers between devices: 33.7 us -> 32.3 us
    all_to_all x1, waiting for transfers between devices: 9.29 us -> 11.2 us  [exchange(): lax.all_to_all(pieces, 'ra', split_axis=0, concat_axis=0, tiled=True, axi...]
where the time goes in v4:
time: 138 us
  blocking collectives  70.9 us (51%)
  starting transfers between devices  32.3 us (23%)
  waiting for transfers between devices  17.5 us (13%)
  Pallas kernels  14.8 us (11%)
    all_to_all x4, blocking collectives, exchange(): lax.all_to_all(pieces, 'ra', split_axis=0, concat_axis=0, tiled=True, axi...  70.9 us
    all_to_all x1, starting transfers between devices, exchange(): lax.all_to_all(pieces, 'ra', split_axis=0, concat_axis=0, tiled=True, axi...  25.9 us
    pallas_call x1, Pallas kernels, first_up(): pl.pallas_call(first_up_body, out_shape=pieces, in_specs=[hbm] * 3, out_s...  14.1 us
    all_to_all x1, waiting for transfers between devices, exchange(): lax.all_to_all(pieces, 'ra', split_axis=0, concat_axis=0, tiled=True, axi...  11.2 us
    ppermute x6, starting transfers between devices, summed_over(): total = total + lax.ppermute(sent, axis, pairs).astype(F32)  6.45 us
    ppermute x6, waiting for transfers between devices, summed_over(): total = total + lax.ppermute(sent, axis, pairs).astype(F32)  6.34 us
  transfers between devices with their start and end apart: 7, of which 6 were waited for; matrix products, arithmetic and copies ran while one was open for 0% of the time, Pallas kernels for 0%

profile of v4, /device:TPU:33, one launch (start us, length us, event | category | flops | bytes accessed | tf_op | source)
XLA Modules:
  0.0 137.7 jit_solution(1141617592046561652)
XLA Ops:
  0.0 14.1 %first_up.1 = bf16[16,72,128]{2,1,0:T(8,128)(2,1)} custom-call(bf16[64,128]{1,0:T(8,128)(2,1)} %h_hbm.1, f32[1,128]{1,0:T(1,128)} %bitcast.3, bf16[128,2048]{1,0:T(8,128)(2,1)} %up_hbm.1), custom_call_target="tpu_custom_call" | custom-call | flops 33554432 | bytes 2097152 | tf_op jit(solution)/shard_map/first_up/pallas_call | solution.py:135
  14.1 25.9 %all-to-all-start = ((bf16[16,72,128]{2,1,0:T(8,128)(2,1)}), bf16[16,72,128]{2,1,0:T(8,128)(2,1)S(1)}, u32[]{:S(2)}, u32[]{:S(2)}) async-start(bf16[16,72,128]{2,1,0:T(8,128)(2,1)} %first_up.1), calls=%async_computation | async-start | bytes 589824 | tf_op jit(solution)/shard_map/all_to_all | solution.py:28
  40.1 0.6 copy-done.5
  40.7 11.2 %all-to-all-done = bf16[16,72,128]{2,1,0:T(8,128)(2,1)S(1)} async-done(((bf16[16,72,128]{2,1,0:T(8,128)(2,1)}), bf16[16,72,128]{2,1,0:T(8,128)(2,1)S(1)}, u32[]{:S(2)}, u32[]{:S(2)}) %all-to-all-start) | async-done | bytes 294944 | tf_op jit(solution)/shard_map/all_to_all | solution.py:28
  52.0 19.6 %all_to_all.26.everyone_ref = bf16[16,64,128]{2,1,0:T(8,128)(2,1)S(1)} all-to-all(bf16[16,64,128]{2,1,0:T(8,128)(2,1)S(1)} %broadcast_in_dim.24), channel_id=1, replica_groups={{112,120,0,8,16,24,32,40,48,56,64,72,80,88,96,104},{113,121,1,9,17,25,3..., dimensions={0} | all-to-all | bytes 524288 | tf_op jit(solution)/shard_map/all_to_all | solution.py:28
  71.6 0.2 down_sums.2
  71.9 3.0 %collective-permute-start.2 = (bf16[64,128]{1,0:T(8,128)(2,1)S(1)}, bf16[64,128]{1,0:T(8,128)(2,1)S(1)}, u32[]{:S(2)}, u32[]{:S(2)}) collective-permute-start(bf16[64,128]{1,0:T(8,128)(2,1)S(1)} %convert_element_type.64), channel_id=1, source_target_pairs={{0,6},{2,0},{4,2},{6,4},{1,7},{3,1},{5,3},{7,5},{8,14},{10,8},{12,... | collective-permute-start | bytes 49160 | tf_op jit(solution)/shard_map/ppermute | solution.py:43
  74.9 0.3 collective-permute-start.1
  75.1 0.7 collective-permute-start
  75.9 3.2 %collective-permute-done.1 = bf16[64,128]{1,0:T(8,128)(2,1)S(1)} collective-permute-done((bf16[64,128]{1,0:T(8,128)(2,1)S(1)}, bf16[64,128]{1,0:T(8,128)(2,1)S(1)}, u32[]{:S(2)}, u32[]{:S(2)}) %collective-permute-start.1) | collective-permute-done | bytes 16416 | tf_op jit(solution)/shard_map/ppermute | solution.py:43
  79.1 0.1 add_convert_fusion.1.h_ref
  79.2 0.3 second_up.1
  79.5 18.5 %all_to_all.27 = bf16[16,72,128]{2,1,0:T(8,128)(2,1)S(1)} all-to-all(bf16[16,72,128]{2,1,0:T(8,128)(2,1)S(1)} %second_up.1), channel_id=1, replica_groups={{112,120,0,8,16,24,32,40,48,56,64,72,80,88,96,104},{113,121,1,9,17,25,3..., dimensions={0} | all-to-all | bytes 589824 | tf_op jit(solution)/shard_map/all_to_all | solution.py:28
  98.1 19.6 %all_to_all.28.everyone_ref = bf16[16,64,128]{2,1,0:T(8,128)(2,1)S(1)} all-to-all(bf16[16,64,128]{2,1,0:T(8,128)(2,1)S(1)} %broadcast_in_dim.25), channel_id=1, replica_groups={{112,120,0,8,16,24,32,40,48,56,64,72,80,88,96,104},{113,121,1,9,17,25,3..., dimensions={0} | all-to-all | bytes 524288 | tf_op jit(solution)/shard_map/all_to_all | solution.py:28
  117.7 0.2 down_sums.3
  118.0 0.1 collective-permute-start.5
  118.1 1.6 %collective-permute-start.4 = (bf16[64,128]{1,0:T(8,128)(2,1)S(1)}, bf16[64,128]{1,0:T(8,128)(2,1)S(1)}, u32[]{:S(2)}, u32[]{:S(2)}) collective-permute-start(bf16[64,128]{1,0:T(8,128)(2,1)S(1)} %convert_element_type.73), channel_id=1, source_target_pairs={{0,4},{2,6},{4,0},{6,2},{1,5},{3,7},{5,1},{7,3},{8,12},{10,14},{12... | collective-permute-start | bytes 49160 | tf_op jit(solution)/shard_map/ppermute | solution.py:43
  119.7 0.7 collective-permute-start.3
  120.4 0.2 collective-permute-done.5
  120.7 1.7 %collective-permute-done.4 = bf16[64,128]{1,0:T(8,128)(2,1)S(1)} collective-permute-done((bf16[64,128]{1,0:T(8,128)(2,1)S(1)}, bf16[64,128]{1,0:T(8,128)(2,1)S(1)}, u32[]{:S(2)}, u32[]{:S(2)}) %collective-permute-start.4) | collective-permute-done | bytes 16416 | tf_op jit(solution)/shard_map/ppermute | solution.py:43
  122.3 1.2 collective-permute-done.3
  123.5 0.2 fusion
  123.7 13.3 %all_to_all.29 = f32[16,1,64]{2,1,0:T(1,128)S(1)} all-to-all(f32[16,1,64]{2,1,0:T(1,128)S(1)} %broadcast_in_dim.26), channel_id=1, replica_groups={{64,72,80,88,96,104,112,120,0,8,16,24,32,40,48,56},{65,73,81,89,97,105,..., dimensions={0} | all-to-all | bytes 8192 | tf_op jit(solution)/shard_map/all_to_all | solution.py:28
  137.0 0.7 fusion.2
  (30 shorter events, 0.4 us)
Async XLA Ops:
  14.1 25.9 %copy-start.4 = (f32[128]{0:T(128)S(1)}, f32[128]{0:T(128)}, u32[]{:S(2)}) copy-start(f32[128]{0:T(128)} %param.12) | copy-start | bytes 1540
  14.1 37.7 %all-to-all-start = ((bf16[16,72,128]{2,1,0:T(8,128)(2,1)}), bf16[16,72,128]{2,1,0:T(8,128)(2,1)S(1)}, u32[]{:S(2)}, u32[]{:S(2)}) async-start(bf16[16,72,128]{2,1,0:T(8,128)(2,1)} %first_up.1), calls=%async_computation | async-start | bytes 589824 | tf_op jit(solution)/shard_map/all_to_all | solution.py:28
  40.0 0.7 copy-start.5
  51.9 19.7 %copy-start = (bf16[2048,128]{1,0:T(8,128)(2,1)S(1)}, bf16[2048,128]{1,0:T(8,128)(2,1)}, u32[]{:S(2)}) copy-start(bf16[2048,128]{1,0:T(8,128)(2,1)} %down_ref.2) | copy-start | bytes 1572868
  71.6 7.6 %copy-start.1 = (bf16[128,2048]{1,0:T(8,128)(2,1)S(1)}, bf16[128,2048]{1,0:T(8,128)(2,1)}, u32[]{:S(2)}) copy-start(bf16[128,2048]{1,0:T(8,128)(2,1)} %up_ref.1) | copy-start | bytes 1572868
  71.8 7.3 %copy-start.3 = (bf16[64,128]{1,0:T(8,128)(2,1)S(1)}, bf16[64,128]{1,0:T(8,128)(2,1)}, u32[]{:S(2)}) copy-start(bf16[64,128]{1,0:T(8,128)(2,1)} %h_hbm.1) | copy-start | bytes 49156
  71.9 4.0 %collective-permute-start.2 = (bf16[64,128]{1,0:T(8,128)(2,1)S(1)}, bf16[64,128]{1,0:T(8,128)(2,1)S(1)}, u32[]{:S(2)}, u32[]{:S(2)}) collective-permute-start(bf16[64,128]{1,0:T(8,128)(2,1)S(1)} %convert_element_type.64), channel_id=1, source_target_pairs={{0,6},{2,0},{4,2},{6,4},{1,7},{3,1},{5,3},{7,5},{8,14},{10,8},{12,... | collective-permute-start | bytes 49160 | tf_op jit(solution)/shard_map/ppermute | solution.py:43
  74.9 4.2 %collective-permute-start.1 = (bf16[64,128]{1,0:T(8,128)(2,1)S(1)}, bf16[64,128]{1,0:T(8,128)(2,1)S(1)}, u32[]{:S(2)}, u32[]{:S(2)}) collective-permute-start(bf16[64,128]{1,0:T(8,128)(2,1)S(1)} %convert_element_type.64), channel_id=1, source_target_pairs={{0,4},{2,6},{4,0},{6,2},{1,5},{3,7},{5,1},{7,3},{8,12},{10,14},{12... | collective-permute-start | bytes 49160 | tf_op jit(solution)/shard_map/ppermute | solution.py:43
  75.1 4.0 %collective-permute-start = (bf16[64,128]{1,0:T(8,128)(2,1)S(1)}, bf16[64,128]{1,0:T(8,128)(2,1)S(1)}, u32[]{:S(2)}, u32[]{:S(2)}) collective-permute-start(bf16[64,128]{1,0:T(8,128)(2,1)S(1)} %convert_element_type.64), channel_id=1, source_target_pairs={{0,2},{2,4},{4,6},{6,0},{1,3},{3,5},{5,7},{7,1},{8,10},{10,12},{12... | collective-permute-start | bytes 49160 | tf_op jit(solution)/shard_map/ppermute | solution.py:43
  98.0 19.7 %copy-start.2 = (bf16[2048,128]{1,0:T(8,128)(2,1)S(1)}, bf16[2048,128]{1,0:T(8,128)(2,1)}, u32[]{:S(2)}) copy-start(bf16[2048,128]{1,0:T(8,128)(2,1)} %down_ref.3) | copy-start | bytes 1572868
  118.0 2.7 %collective-permute-start.5 = (bf16[64,128]{1,0:T(8,128)(2,1)S(1)}, bf16[64,128]{1,0:T(8,128)(2,1)S(1)}, u32[]{:S(2)}, u32[]{:S(2)}) collective-permute-start(bf16[64,128]{1,0:T(8,128)(2,1)S(1)} %convert_element_type.73), channel_id=1, source_target_pairs={{0,6},{2,0},{4,2},{6,4},{1,7},{3,1},{5,3},{7,5},{8,14},{10,8},{12,... | collective-permute-start | bytes 49160 | tf_op jit(solution)/shard_map/ppermute | solution.py:43
  118.1 4.2 %collective-permute-start.4 = (bf16[64,128]{1,0:T(8,128)(2,1)S(1)}, bf16[64,128]{1,0:T(8,128)(2,1)S(1)}, u32[]{:S(2)}, u32[]{:S(2)}) collective-permute-start(bf16[64,128]{1,0:T(8,128)(2,1)S(1)} %convert_element_type.73), channel_id=1, source_target_pairs={{0,4},{2,6},{4,0},{6,2},{1,5},{3,7},{5,1},{7,3},{8,12},{10,14},{12... | collective-permute-start | bytes 49160 | tf_op jit(solution)/shard_map/ppermute | solution.py:43
  119.7 3.8 %collective-permute-start.3 = (bf16[64,128]{1,0:T(8,128)(2,1)S(1)}, bf16[64,128]{1,0:T(8,128)(2,1)S(1)}, u32[]{:S(2)}, u32[]{:S(2)}) collective-permute-start(bf16[64,128]{1,0:T(8,128)(2,1)S(1)} %convert_element_type.73), channel_id=1, source_target_pairs={{0,2},{2,4},{4,6},{6,0},{1,3},{3,5},{5,7},{7,1},{8,10},{10,12},{12... | collective-permute-start | bytes 49160 | tf_op jit(solution)/shard_map/ppermute | solution.py:43

commit v5 on v4

--- a/solution.py
+++ b/solution.py
@@ -8,7 +8,7 @@
 EPS = 1e-06
 F32 = jnp.float32
 BF16 = jnp.bfloat16
-STAGGER_NS = 12800
+STAGGER_NS = 12700
 STAGGER_CORE = 1
 LEAD_EIGHTHS = 7
 LAST_LEAD_EIGHTHS = 4
@@ -39,7 +39,7 @@
     total = value
     sent = value.astype(SUM_TYPE)
     for step in range(1, size):
-        pairs = [(i, (i + step) % size) for i in range(size)]
+        pairs = [(i, i ^ step) for i in range(size)]
         total = total + lax.ppermute(sent, axis, pairs).astype(F32)
     return total
 

time: 138 us -> 137 us (level)
  transfers between devices with their start and end apart: 7 -> 7, of which waited for: 6 -> 5; matrix products, arithmetic and copies ran while one was open for 0% -> 0% of each run, Pallas kernels for 0% -> 0%
where the time goes in v5:
time: 137 us
  blocking collectives  71 us (52%)
  starting transfers between devices  33 us (24%)
  waiting for transfers between devices  16.3 us (12%)
  Pallas kernels  14.7 us (11%)
    all_to_all x4, blocking collectives, exchange(): lax.all_to_all(pieces, 'ra', split_axis=0, concat_axis=0, tiled=True, axi...  71 us
    all_to_all x1, starting transfers between devices, exchange(): lax.all_to_all(pieces, 'ra', split_axis=0, concat_axis=0, tiled=True, axi...  25.9 us
    pallas_call x1, Pallas kernels, first_up(): pl.pallas_call(first_up_body, out_shape=pieces, in_specs=[hbm] * 3, out_s...  14 us
    all_to_all x1, waiting for transfers between devices, exchange(): lax.all_to_all(pieces, 'ra', split_axis=0, concat_axis=0, tiled=True, axi...  11.2 us
    ppermute x6, starting transfers between devices, summed_over(): total = total + lax.ppermute(sent, axis, pairs).astype(F32)  7.11 us
    ppermute x6, waiting for transfers between devices, summed_over(): total = total + lax.ppermute(sent, axis, pairs).astype(F32)  5.15 us
  transfers between devices with their start and end apart: 7, of which 5 were waited for; matrix products, arithmetic and copies ran while one was open for 0% of the time, Pallas kernels for 0%

profile of v5, /device:TPU:33, one launch (start us, length us, event | category | flops | bytes accessed | tf_op | source)
XLA Modules:
  0.0 137.1 jit_solution(6564252170029032496)
XLA Ops:
  0.0 14.0 %first_up.1 = bf16[16,72,128]{2,1,0:T(8,128)(2,1)} custom-call(bf16[64,128]{1,0:T(8,128)(2,1)} %h_hbm.1, f32[1,128]{1,0:T(1,128)} %bitcast.3, bf16[128,2048]{1,0:T(8,128)(2,1)} %up_hbm.1), custom_call_target="tpu_custom_call" | custom-call | flops 33554432 | bytes 2097152 | tf_op jit(solution)/shard_map/first_up/pallas_call | solution.py:135
  14.0 25.9 %all-to-all-start = ((bf16[16,72,128]{2,1,0:T(8,128)(2,1)}), bf16[16,72,128]{2,1,0:T(8,128)(2,1)S(1)}, u32[]{:S(2)}, u32[]{:S(2)}) async-start(bf16[16,72,128]{2,1,0:T(8,128)(2,1)} %first_up.1), calls=%async_computation | async-start | bytes 589824 | tf_op jit(solution)/shard_map/all_to_all | solution.py:28
  39.9 0.6 copy-done.5
  40.6 11.2 %all-to-all-done = bf16[16,72,128]{2,1,0:T(8,128)(2,1)S(1)} async-done(((bf16[16,72,128]{2,1,0:T(8,128)(2,1)}), bf16[16,72,128]{2,1,0:T(8,128)(2,1)S(1)}, u32[]{:S(2)}, u32[]{:S(2)}) %all-to-all-start) | async-done | bytes 294944 | tf_op jit(solution)/shard_map/all_to_all | solution.py:28
  51.9 19.6 %all_to_all.26.everyone_ref = bf16[16,64,128]{2,1,0:T(8,128)(2,1)S(1)} all-to-all(bf16[16,64,128]{2,1,0:T(8,128)(2,1)S(1)} %broadcast_in_dim.24), channel_id=1, replica_groups={{112,120,0,8,16,24,32,40,48,56,64,72,80,88,96,104},{113,121,1,9,17,25,3..., dimensions={0} | all-to-all | bytes 524288 | tf_op jit(solution)/shard_map/all_to_all | solution.py:28
  71.5 0.2 down_sums.2
  71.8 3.0 %collective-permute-start.2 = (bf16[64,128]{1,0:T(8,128)(2,1)S(1)}, bf16[64,128]{1,0:T(8,128)(2,1)S(1)}, u32[]{:S(2)}, u32[]{:S(2)}) collective-permute-start(bf16[64,128]{1,0:T(8,128)(2,1)S(1)} %convert_element_type.64), channel_id=1, source_target_pairs={{0,6},{2,4},{4,2},{6,0},{1,7},{3,5},{5,3},{7,1},{8,14},{10,12},{12... | collective-permute-start | bytes 49160 | tf_op jit(solution)/shard_map/ppermute | solution.py:43
  74.8 0.3 collective-permute-start.1
  75.0 0.4 collective-permute-start
  75.5 0.4 collective-permute-done.2
  75.9 3.0 %collective-permute-done.1 = bf16[64,128]{1,0:T(8,128)(2,1)S(1)} collective-permute-done((bf16[64,128]{1,0:T(8,128)(2,1)S(1)}, bf16[64,128]{1,0:T(8,128)(2,1)S(1)}, u32[]{:S(2)}, u32[]{:S(2)}) %collective-permute-start.1) | collective-permute-done | bytes 16416 | tf_op jit(solution)/shard_map/ppermute | solution.py:43
  78.9 0.1 add_convert_fusion.1.h_ref
  79.0 0.3 second_up.1
  79.2 18.5 %all_to_all.27 = bf16[16,72,128]{2,1,0:T(8,128)(2,1)S(1)} all-to-all(bf16[16,72,128]{2,1,0:T(8,128)(2,1)S(1)} %second_up.1), channel_id=1, replica_groups={{112,120,0,8,16,24,32,40,48,56,64,72,80,88,96,104},{113,121,1,9,17,25,3..., dimensions={0} | all-to-all | bytes 589824 | tf_op jit(solution)/shard_map/all_to_all | solution.py:28
  97.9 19.6 %all_to_all.28.everyone_ref = bf16[16,64,128]{2,1,0:T(8,128)(2,1)S(1)} all-to-all(bf16[16,64,128]{2,1,0:T(8,128)(2,1)S(1)} %broadcast_in_dim.25), channel_id=1, replica_groups={{112,120,0,8,16,24,32,40,48,56,64,72,80,88,96,104},{113,121,1,9,17,25,3..., dimensions={0} | all-to-all | bytes 524288 | tf_op jit(solution)/shard_map/all_to_all | solution.py:28
  117.5 0.2 down_sums.3
  117.8 1.1 collective-permute-start.5
  118.8 0.9 collective-permute-start.4
  119.7 1.4 %collective-permute-start.3 = (bf16[64,128]{1,0:T(8,128)(2,1)S(1)}, bf16[64,128]{1,0:T(8,128)(2,1)S(1)}, u32[]{:S(2)}, u32[]{:S(2)}) collective-permute-start(bf16[64,128]{1,0:T(8,128)(2,1)S(1)} %convert_element_type.73), channel_id=1, source_target_pairs={{0,2},{2,0},{4,6},{6,4},{1,3},{3,1},{5,7},{7,5},{8,10},{10,8},{12,... | collective-permute-start | bytes 49160 | tf_op jit(solution)/shard_map/ppermute | solution.py:43
  121.1 0.5 collective-permute-done.5
  121.7 1.2 collective-permute-done.4
  122.9 0.2 fusion
  123.1 13.3 %all_to_all.29 = f32[16,1,64]{2,1,0:T(1,128)S(1)} all-to-all(f32[16,1,64]{2,1,0:T(1,128)S(1)} %broadcast_in_dim.26), channel_id=1, replica_groups={{64,72,80,88,96,104,112,120,0,8,16,24,32,40,48,56},{65,73,81,89,97,105,..., dimensions={0} | all-to-all | bytes 8192 | tf_op jit(solution)/shard_map/all_to_all | solution.py:28
  136.4 0.7 fusion.2
  (30 shorter events, 0.4 us)
Async XLA Ops:
  14.0 25.9 %copy-start.4 = (f32[128]{0:T(128)S(1)}, f32[128]{0:T(128)}, u32[]{:S(2)}) copy-start(f32[128]{0:T(128)} %param.12) | copy-start | bytes 1540
  14.0 37.7 %all-to-all-start = ((bf16[16,72,128]{2,1,0:T(8,128)(2,1)}), bf16[16,72,128]{2,1,0:T(8,128)(2,1)S(1)}, u32[]{:S(2)}, u32[]{:S(2)}) async-start(bf16[16,72,128]{2,1,0:T(8,128)(2,1)} %first_up.1), calls=%async_computation | async-start | bytes 589824 | tf_op jit(solution)/shard_map/all_to_all | solution.py:28
  39.9 0.7 copy-start.5
  51.8 19.7 %copy-start = (bf16[2048,128]{1,0:T(8,128)(2,1)S(1)}, bf16[2048,128]{1,0:T(8,128)(2,1)}, u32[]{:S(2)}) copy-start(bf16[2048,128]{1,0:T(8,128)(2,1)} %down_ref.2) | copy-start | bytes 1572868
  71.5 7.5 %copy-start.1 = (bf16[128,2048]{1,0:T(8,128)(2,1)S(1)}, bf16[128,2048]{1,0:T(8,128)(2,1)}, u32[]{:S(2)}) copy-start(bf16[128,2048]{1,0:T(8,128)(2,1)} %up_ref.1) | copy-start | bytes 1572868
  71.7 7.1 %copy-start.3 = (bf16[64,128]{1,0:T(8,128)(2,1)S(1)}, bf16[64,128]{1,0:T(8,128)(2,1)}, u32[]{:S(2)}) copy-start(bf16[64,128]{1,0:T(8,128)(2,1)} %h_hbm.1) | copy-start | bytes 49156
  71.8 4.2 %collective-permute-start.2 = (bf16[64,128]{1,0:T(8,128)(2,1)S(1)}, bf16[64,128]{1,0:T(8,128)(2,1)S(1)}, u32[]{:S(2)}, u32[]{:S(2)}) collective-permute-start(bf16[64,128]{1,0:T(8,128)(2,1)S(1)} %convert_element_type.64), channel_id=1, source_target_pairs={{0,6},{2,4},{4,2},{6,0},{1,7},{3,5},{5,3},{7,1},{8,14},{10,12},{12... | collective-permute-start | bytes 49160 | tf_op jit(solution)/shard_map/ppermute | solution.py:43
  74.8 4.1 %collective-permute-start.1 = (bf16[64,128]{1,0:T(8,128)(2,1)S(1)}, bf16[64,128]{1,0:T(8,128)(2,1)S(1)}, u32[]{:S(2)}, u32[]{:S(2)}) collective-permute-start(bf16[64,128]{1,0:T(8,128)(2,1)S(1)} %convert_element_type.64), channel_id=1, source_target_pairs={{0,4},{2,6},{4,0},{6,2},{1,5},{3,7},{5,1},{7,3},{8,12},{10,14},{12... | collective-permute-start | bytes 49160 | tf_op jit(solution)/shard_map/ppermute | solution.py:43
  75.0 3.8 %collective-permute-start = (bf16[64,128]{1,0:T(8,128)(2,1)S(1)}, bf16[64,128]{1,0:T(8,128)(2,1)S(1)}, u32[]{:S(2)}, u32[]{:S(2)}) collective-permute-start(bf16[64,128]{1,0:T(8,128)(2,1)S(1)} %convert_element_type.64), channel_id=1, source_target_pairs={{0,2},{2,0},{4,6},{6,4},{1,3},{3,1},{5,7},{7,5},{8,10},{10,8},{12,... | collective-permute-start | bytes 49160 | tf_op jit(solution)/shard_map/ppermute | solution.py:43
  97.8 19.8 %copy-start.2 = (bf16[2048,128]{1,0:T(8,128)(2,1)S(1)}, bf16[2048,128]{1,0:T(8,128)(2,1)}, u32[]{:S(2)}) copy-start(bf16[2048,128]{1,0:T(8,128)(2,1)} %down_ref.3) | copy-start | bytes 1572868
  117.8 3.9 %collective-permute-start.5 = (bf16[64,128]{1,0:T(8,128)(2,1)S(1)}, bf16[64,128]{1,0:T(8,128)(2,1)S(1)}, u32[]{:S(2)}, u32[]{:S(2)}) collective-permute-start(bf16[64,128]{1,0:T(8,128)(2,1)S(1)} %convert_element_type.73), channel_id=1, source_target_pairs={{0,6},{2,4},{4,2},{6,0},{1,7},{3,5},{5,3},{7,1},{8,14},{10,12},{12... | collective-permute-start | bytes 49160 | tf_op jit(solution)/shard_map/ppermute | solution.py:43
  118.8 4.1 %collective-permute-start.4 = (bf16[64,128]{1,0:T(8,128)(2,1)S(1)}, bf16[64,128]{1,0:T(8,128)(2,1)S(1)}, u32[]{:S(2)}, u32[]{:S(2)}) collective-permute-start(bf16[64,128]{1,0:T(8,128)(2,1)S(1)} %convert_element_type.73), channel_id=1, source_target_pairs={{0,4},{2,6},{4,0},{6,2},{1,5},{3,7},{5,1},{7,3},{8,12},{10,14},{12... | collective-permute-start | bytes 49160 | tf_op jit(solution)/shard_map/ppermute | solution.py:43
  119.7 3.2 %collective-permute-start.3 = (bf16[64,128]{1,0:T(8,128)(2,1)S(1)}, bf16[64,128]{1,0:T(8,128)(2,1)S(1)}, u32[]{:S(2)}, u32[]{:S(2)}) collective-permute-start(bf16[64,128]{1,0:T(8,128)(2,1)S(1)} %convert_element_type.73), channel_id=1, source_target_pairs={{0,2},{2,0},{4,6},{6,4},{1,3},{3,1},{5,7},{7,5},{8,10},{10,8},{12,... | collective-permute-start | bytes 49160 | tf_op jit(solution)/shard_map/ppermute | solution.py:43

commit v6 on v5

--- a/solution.py
+++ b/solution.py
@@ -8,11 +8,10 @@
 EPS = 1e-06
 F32 = jnp.float32
 BF16 = jnp.bfloat16
-STAGGER_NS = 12700
+STAGGER_NS = 13200
 STAGGER_CORE = 1
 LEAD_EIGHTHS = 7
 LAST_LEAD_EIGHTHS = 4
-SUM_TYPE = BF16
 UP_COST = 2 << 20
 PAD = 8
 CHUNKS = 2
@@ -34,10 +33,8 @@
     return exchange(jnp.broadcast_to(shard, (lax.axis_size("ra"), *shard.shape)), eighths)
 
 
-def summed_over(value, axis):
+def summed_over(total, sent, axis):
     size = lax.axis_size(axis)
-    total = value
-    sent = value.astype(SUM_TYPE)
     for step in range(1, size):
         pairs = [(i, i ^ step) for i in range(size)]
         total = total + lax.ppermute(sent, axis, pairs).astype(F32)
@@ -162,7 +159,7 @@
     )(h, gain, w_up)
 
 
-def down_body(everyone_ref, down_ref, out_ref):
+def down_body(everyone_ref, down_ref, out_ref, sent_ref):
     rows, lanes = out_ref.shape[0], everyone_ref.shape[2]
     order = member_order(everyone_ref.shape[0])
     total = jnp.zeros(out_ref.shape, F32)
@@ -173,12 +170,13 @@
             jnp.concatenate(pair, axis=1), weights, preferred_element_type=F32
         )
     out_ref[...] = total
+    sent_ref[...] = total.astype(BF16)
 
 
 def down_sums(everyone, w_down, rows):
     return pl.pallas_call(
         down_body,
-        out_shape=jax.ShapeDtypeStruct((rows, w_down.shape[1]), F32),
+        out_shape=[jax.ShapeDtypeStruct((rows, w_down.shape[1]), kind) for kind in (F32, BF16)],
         compiler_params=pltpu.CompilerParams(vmem_limit_bytes=8 * 1024 * 1024),
         cost_estimate=pl.CostEstimate(
             flops=2 * rows * w_down.size, bytes_accessed=UP_COST, transcendentals=0
@@ -197,8 +195,7 @@
     hidden_share, squares = lax.optimization_barrier((hidden_share, squares))
     everyone = sent_to_all(hidden_share)
     mean_sq = squares / (ra * w_down.shape[1])
-    down = down_sums(everyone, w_down, rows)
-    return summed_over(down, "cb") / (mean_sq + EPS)[:, None], beside
+    return summed_over(*down_sums(everyone, w_down, rows), "cb") / (mean_sq + EPS)[:, None], beside
 
 
 def local(tokens, gain_first, up_first, down_first, gain_second, up_second, down_second, gain_last):

time: 137 us -> 138 us (level)
  no operation moved by 1% of the time
where the time goes in v6:
time: 138 us
  blocking collectives  70.4 us (51%)
  starting transfers between devices  33 us (24%)
  waiting for transfers between devices  16.8 us (12%)
  Pallas kernels  15.2 us (11%)
    all_to_all x4, blocking collectives, exchange(): lax.all_to_all(pieces, 'ra', split_axis=0, concat_axis=0, tiled=True, axi...  70.4 us
    all_to_all x1, starting transfers between devices, exchange(): lax.all_to_all(pieces, 'ra', split_axis=0, concat_axis=0, tiled=True, axi...  25.9 us
    pallas_call x1, Pallas kernels, first_up(): pl.pallas_call(first_up_body, out_shape=pieces, in_specs=[hbm] * 3, out_s...  14.5 us
    all_to_all x1, waiting for transfers between devices, exchange(): lax.all_to_all(pieces, 'ra', split_axis=0, concat_axis=0, tiled=True, axi...  11.2 us
    ppermute x6, starting transfers between devices, summed_over(): total = total + lax.ppermute(sent, axis, pairs).astype(F32)  7.11 us
    ppermute x6, waiting for transfers between devices, summed_over(): total = total + lax.ppermute(sent, axis, pairs).astype(F32)  5.6 us
  transfers between devices with their start and end apart: 7, of which 5 were waited for; matrix products, arithmetic and copies ran while one was open for 0% of the time, Pallas kernels for 0%

profile of v6, /device:TPU:33, one launch (start us, length us, event | category | flops | bytes accessed | tf_op | source)
XLA Modules:
  0.0 137.5 jit_solution(673659712967351883)
XLA Ops:
  0.0 14.5 %first_up.1 = bf16[16,72,128]{2,1,0:T(8,128)(2,1)} custom-call(bf16[64,128]{1,0:T(8,128)(2,1)} %h_hbm.1, f32[1,128]{1,0:T(1,128)} %bitcast.3, bf16[128,2048]{1,0:T(8,128)(2,1)} %up_hbm.1), custom_call_target="tpu_custom_call" | custom-call | flops 33554432 | bytes 2097152 | tf_op jit(solution)/shard_map/first_up/pallas_call | solution.py:132
  14.5 25.9 %all-to-all-start = ((bf16[16,72,128]{2,1,0:T(8,128)(2,1)}), bf16[16,72,128]{2,1,0:T(8,128)(2,1)S(1)}, u32[]{:S(2)}, u32[]{:S(2)}) async-start(bf16[16,72,128]{2,1,0:T(8,128)(2,1)} %first_up.1), calls=%async_computation | async-start | bytes 589824 | tf_op jit(solution)/shard_map/all_to_all | solution.py:27
  40.5 0.6 copy-done.5
  41.1 11.2 %all-to-all-done = bf16[16,72,128]{2,1,0:T(8,128)(2,1)S(1)} async-done(((bf16[16,72,128]{2,1,0:T(8,128)(2,1)}), bf16[16,72,128]{2,1,0:T(8,128)(2,1)S(1)}, u32[]{:S(2)}, u32[]{:S(2)}) %all-to-all-start) | async-done | bytes 294944 | tf_op jit(solution)/shard_map/all_to_all | solution.py:27
  52.4 19.6 %all_to_all.26.everyone_ref = bf16[16,64,128]{2,1,0:T(8,128)(2,1)S(1)} all-to-all(bf16[16,64,128]{2,1,0:T(8,128)(2,1)S(1)} %broadcast_in_dim.24), channel_id=1, replica_groups={{112,120,0,8,16,24,32,40,48,56,64,72,80,88,96,104},{113,121,1,9,17,25,3..., dimensions={0} | all-to-all | bytes 524288 | tf_op jit(solution)/shard_map/all_to_all | solution.py:27
  72.0 0.2 down_sums.2
  72.2 3.0 %collective-permute-start.2 = (bf16[64,128]{1,0:T(8,128)(2,1)S(1)}, bf16[64,128]{1,0:T(8,128)(2,1)S(1)}, u32[]{:S(2)}, u32[]{:S(2)}) collective-permute-start(bf16[64,128]{1,0:T(8,128)(2,1)S(1)} %get-tuple-element.33), channel_id=1, source_target_pairs={{0,6},{2,4},{4,2},{6,0},{1,7},{3,5},{5,3},{7,1},{8,14},{10,12},{12... | collective-permute-start | bytes 49160 | tf_op jit(solution)/shard_map/ppermute | solution.py:40
  75.2 0.3 collective-permute-start.1
  75.5 0.4 collective-permute-start
  76.0 0.4 collective-permute-done.2
  76.4 3.0 %collective-permute-done.1 = bf16[64,128]{1,0:T(8,128)(2,1)S(1)} collective-permute-done((bf16[64,128]{1,0:T(8,128)(2,1)S(1)}, bf16[64,128]{1,0:T(8,128)(2,1)S(1)}, u32[]{:S(2)}, u32[]{:S(2)}) %collective-permute-start.1) | collective-permute-done | bytes 16416 | tf_op jit(solution)/shard_map/ppermute | solution.py:40
  79.3 0.1 add_convert_fusion.1.h_ref
  79.5 0.3 second_up.1
  79.7 18.5 %all_to_all.27 = bf16[16,72,128]{2,1,0:T(8,128)(2,1)S(1)} all-to-all(bf16[16,72,128]{2,1,0:T(8,128)(2,1)S(1)} %second_up.1), channel_id=1, replica_groups={{112,120,0,8,16,24,32,40,48,56,64,72,80,88,96,104},{113,121,1,9,17,25,3..., dimensions={0} | all-to-all | bytes 589824 | tf_op jit(solution)/shard_map/all_to_all | solution.py:27
  98.4 18.4 %all_to_all.28.everyone_ref = bf16[16,64,128]{2,1,0:T(8,128)(2,1)S(1)} all-to-all(bf16[16,64,128]{2,1,0:T(8,128)(2,1)S(1)} %broadcast_in_dim.25), channel_id=1, replica_groups={{112,120,0,8,16,24,32,40,48,56,64,72,80,88,96,104},{113,121,1,9,17,25,3..., dimensions={0} | all-to-all | bytes 524288 | tf_op jit(solution)/shard_map/all_to_all | solution.py:27
  116.8 0.2 down_sums.3
  117.0 1.5 %collective-permute-start.5 = (bf16[64,128]{1,0:T(8,128)(2,1)S(1)}, bf16[64,128]{1,0:T(8,128)(2,1)S(1)}, u32[]{:S(2)}, u32[]{:S(2)}) collective-permute-start(bf16[64,128]{1,0:T(8,128)(2,1)S(1)} %get-tuple-element.40), channel_id=1, source_target_pairs={{0,6},{2,4},{4,2},{6,0},{1,7},{3,5},{5,3},{7,1},{8,14},{10,12},{12... | collective-permute-start | bytes 49160 | tf_op jit(solution)/shard_map/ppermute | solution.py:40
  118.5 0.9 collective-permute-start.4
  119.4 0.9 collective-permute-start.3
  120.4 0.5 collective-permute-done.5
  120.9 1.7 %collective-permute-done.4 = bf16[64,128]{1,0:T(8,128)(2,1)S(1)} collective-permute-done((bf16[64,128]{1,0:T(8,128)(2,1)S(1)}, bf16[64,128]{1,0:T(8,128)(2,1)S(1)}, u32[]{:S(2)}, u32[]{:S(2)}) %collective-permute-start.4) | collective-permute-done | bytes 16416 | tf_op jit(solution)/shard_map/ppermute | solution.py:40
  122.6 0.2 fusion
  122.8 14.0 %all_to_all.29 = f32[16,1,64]{2,1,0:T(1,128)S(1)} all-to-all(f32[16,1,64]{2,1,0:T(1,128)S(1)} %broadcast_in_dim.26), channel_id=1, replica_groups={{64,72,80,88,96,104,112,120,0,8,16,24,32,40,48,56},{65,73,81,89,97,105,..., dimensions={0} | all-to-all | bytes 8192 | tf_op jit(solution)/shard_map/all_to_all | solution.py:27
  136.8 0.7 fusion.2
  (28 shorter events, 0.3 us)
Async XLA Ops:
  14.5 25.9 %copy-start.4 = (f32[128]{0:T(128)S(1)}, f32[128]{0:T(128)}, u32[]{:S(2)}) copy-start(f32[128]{0:T(128)} %param.12) | copy-start | bytes 1540
  14.5 37.7 %all-to-all-start = ((bf16[16,72,128]{2,1,0:T(8,128)(2,1)}), bf16[16,72,128]{2,1,0:T(8,128)(2,1)S(1)}, u32[]{:S(2)}, u32[]{:S(2)}) async-start(bf16[16,72,128]{2,1,0:T(8,128)(2,1)} %first_up.1), calls=%async_computation | async-start | bytes 589824 | tf_op jit(solution)/shard_map/all_to_all | solution.py:27
  40.4 0.7 copy-start.5
  52.3 19.7 %copy-start = (bf16[2048,128]{1,0:T(8,128)(2,1)S(1)}, bf16[2048,128]{1,0:T(8,128)(2,1)}, u32[]{:S(2)}) copy-start(bf16[2048,128]{1,0:T(8,128)(2,1)} %down_ref.2) | copy-start | bytes 1572868
  72.0 7.3 %copy-start.3 = (bf16[64,128]{1,0:T(8,128)(2,1)S(1)}, bf16[64,128]{1,0:T(8,128)(2,1)}, u32[]{:S(2)}) copy-start(bf16[64,128]{1,0:T(8,128)(2,1)} %h_hbm.1) | copy-start | bytes 49156
  72.0 7.4 %copy-start.2 = (bf16[128,2048]{1,0:T(8,128)(2,1)S(1)}, bf16[128,2048]{1,0:T(8,128)(2,1)}, u32[]{:S(2)}) copy-start(bf16[128,2048]{1,0:T(8,128)(2,1)} %up_ref.1) | copy-start | bytes 1572868
  72.2 4.2 %collective-permute-start.2 = (bf16[64,128]{1,0:T(8,128)(2,1)S(1)}, bf16[64,128]{1,0:T(8,128)(2,1)S(1)}, u32[]{:S(2)}, u32[]{:S(2)}) collective-permute-start(bf16[64,128]{1,0:T(8,128)(2,1)S(1)} %get-tuple-element.33), channel_id=1, source_target_pairs={{0,6},{2,4},{4,2},{6,0},{1,7},{3,5},{5,3},{7,1},{8,14},{10,12},{12... | collective-permute-start | bytes 49160 | tf_op jit(solution)/shard_map/ppermute | solution.py:40
  75.2 4.1 %collective-permute-start.1 = (bf16[64,128]{1,0:T(8,128)(2,1)S(1)}, bf16[64,128]{1,0:T(8,128)(2,1)S(1)}, u32[]{:S(2)}, u32[]{:S(2)}) collective-permute-start(bf16[64,128]{1,0:T(8,128)(2,1)S(1)} %get-tuple-element.33), channel_id=1, source_target_pairs={{0,4},{2,6},{4,0},{6,2},{1,5},{3,7},{5,1},{7,3},{8,12},{10,14},{12... | collective-permute-start | bytes 49160 | tf_op jit(solution)/shard_map/ppermute | solution.py:40
  75.5 3.8 %collective-permute-start = (bf16[64,128]{1,0:T(8,128)(2,1)S(1)}, bf16[64,128]{1,0:T(8,128)(2,1)S(1)}, u32[]{:S(2)}, u32[]{:S(2)}) collective-permute-start(bf16[64,128]{1,0:T(8,128)(2,1)S(1)} %get-tuple-element.33), channel_id=1, source_target_pairs={{0,2},{2,0},{4,6},{6,4},{1,3},{3,1},{5,7},{7,5},{8,10},{10,8},{12,... | collective-permute-start | bytes 49160 | tf_op jit(solution)/shard_map/ppermute | solution.py:40
  98.3 18.5 %copy-start.1 = (bf16[2048,128]{1,0:T(8,128)(2,1)S(1)}, bf16[2048,128]{1,0:T(8,128)(2,1)}, u32[]{:S(2)}) copy-start(bf16[2048,128]{1,0:T(8,128)(2,1)} %down_ref.3) | copy-start | bytes 1572868
  117.0 3.9 %collective-permute-start.5 = (bf16[64,128]{1,0:T(8,128)(2,1)S(1)}, bf16[64,128]{1,0:T(8,128)(2,1)S(1)}, u32[]{:S(2)}, u32[]{:S(2)}) collective-permute-start(bf16[64,128]{1,0:T(8,128)(2,1)S(1)} %get-tuple-element.40), channel_id=1, source_target_pairs={{0,6},{2,4},{4,2},{6,0},{1,7},{3,5},{5,3},{7,1},{8,14},{10,12},{12... | collective-permute-start | bytes 49160 | tf_op jit(solution)/shard_map/ppermute | solution.py:40
  118.5 4.1 %collective-permute-start.4 = (bf16[64,128]{1,0:T(8,128)(2,1)S(1)}, bf16[64,128]{1,0:T(8,128)(2,1)S(1)}, u32[]{:S(2)}, u32[]{:S(2)}) collective-permute-start(bf16[64,128]{1,0:T(8,128)(2,1)S(1)} %get-tuple-element.40), channel_id=1, source_target_pairs={{0,4},{2,6},{4,0},{6,2},{1,5},{3,7},{5,1},{7,3},{8,12},{10,14},{12... | collective-permute-start | bytes 49160 | tf_op jit(solution)/shard_map/ppermute | solution.py:40
  119.4 3.2 %collective-permute-start.3 = (bf16[64,128]{1,0:T(8,128)(2,1)S(1)}, bf16[64,128]{1,0:T(8,128)(2,1)S(1)}, u32[]{:S(2)}, u32[]{:S(2)}) collective-permute-start(bf16[64,128]{1,0:T(8,128)(2,1)S(1)} %get-tuple-element.40), channel_id=1, source_target_pairs={{0,2},{2,0},{4,6},{6,4},{1,3},{3,1},{5,7},{7,5},{8,10},{10,8},{12,... | collective-permute-start | bytes 49160 | tf_op jit(solution)/shard_map/ppermute | solution.py:40

commit v7 on v5

--- a/solution.py
+++ b/solution.py
@@ -8,7 +8,7 @@
 EPS = 1e-06
 F32 = jnp.float32
 BF16 = jnp.bfloat16
-STAGGER_NS = 12700
+STAGGER_NS = 13300
 STAGGER_CORE = 1
 LEAD_EIGHTHS = 7
 LAST_LEAD_EIGHTHS = 4

time: 137 us -> 137 us (level)
  transfers between devices with their start and end apart: 7 -> 7, of which waited for: 5 -> 6; matrix products, arithmetic and copies ran while one was open for 0% -> 0% of each run, Pallas kernels for 0% -> 0%
where the time goes in v7:
time: 137 us
  blocking collectives  69.7 us (51%)
  starting transfers between devices  33 us (24%)
  waiting for transfers between devices  16.7 us (12%)
  Pallas kernels  15.3 us (11%)
    all_to_all x4, blocking collectives, exchange(): lax.all_to_all(pieces, 'ra', split_axis=0, concat_axis=0, tiled=True, axi...  69.7 us
    all_to_all x1, starting transfers between devices, exchange(): lax.all_to_all(pieces, 'ra', split_axis=0, concat_axis=0, tiled=True, axi...  25.9 us
    pallas_call x1, Pallas kernels, first_up(): pl.pallas_call(first_up_body, out_shape=pieces, in_specs=[hbm] * 3, out_s...  14.6 us
    all_to_all x1, waiting for transfers between devices, exchange(): lax.all_to_all(pieces, 'ra', split_axis=0, concat_axis=0, tiled=True, axi...  11.2 us
    ppermute x6, starting transfers between devices, summed_over(): total = total + lax.ppermute(sent, axis, pairs).astype(F32)  7.11 us
    ppermute x6, waiting for transfers between devices, summed_over(): total = total + lax.ppermute(sent, axis, pairs).astype(F32)  5.49 us
  transfers between devices with their start and end apart: 7, of which 6 were waited for; matrix products, arithmetic and copies ran while one was open for 0% of the time, Pallas kernels for 0%

profile of v7, /device:TPU:33, one launch (start us, length us, event | category | flops | bytes accessed | tf_op | source)
XLA Modules:
  0.0 136.8 jit_solution(10115972462386180133)
XLA Ops:
  0.0 14.6 %first_up.1 = bf16[16,72,128]{2,1,0:T(8,128)(2,1)} custom-call(bf16[64,128]{1,0:T(8,128)(2,1)} %h_hbm.1, f32[1,128]{1,0:T(1,128)} %bitcast.3, bf16[128,2048]{1,0:T(8,128)(2,1)} %up_hbm.1), custom_call_target="tpu_custom_call" | custom-call | flops 33554432 | bytes 2097152 | tf_op jit(solution)/shard_map/first_up/pallas_call | solution.py:135
  14.7 25.9 %all-to-all-start = ((bf16[16,72,128]{2,1,0:T(8,128)(2,1)}), bf16[16,72,128]{2,1,0:T(8,128)(2,1)S(1)}, u32[]{:S(2)}, u32[]{:S(2)}) async-start(bf16[16,72,128]{2,1,0:T(8,128)(2,1)} %first_up.1), calls=%async_computation | async-start | bytes 589824 | tf_op jit(solution)/shard_map/all_to_all | solution.py:28
  40.5 0.6 copy-done.5
  41.2 11.2 %all-to-all-done = bf16[16,72,128]{2,1,0:T(8,128)(2,1)S(1)} async-done(((bf16[16,72,128]{2,1,0:T(8,128)(2,1)}), bf16[16,72,128]{2,1,0:T(8,128)(2,1)S(1)}, u32[]{:S(2)}, u32[]{:S(2)}) %all-to-all-start) | async-done | bytes 294944 | tf_op jit(solution)/shard_map/all_to_all | solution.py:28
  52.5 19.6 %all_to_all.26.everyone_ref = bf16[16,64,128]{2,1,0:T(8,128)(2,1)S(1)} all-to-all(bf16[16,64,128]{2,1,0:T(8,128)(2,1)S(1)} %broadcast_in_dim.24), channel_id=1, replica_groups={{112,120,0,8,16,24,32,40,48,56,64,72,80,88,96,104},{113,121,1,9,17,25,3..., dimensions={0} | all-to-all | bytes 524288 | tf_op jit(solution)/shard_map/all_to_all | solution.py:28
  72.1 0.2 down_sums.2
  72.4 3.0 %collective-permute-start.2 = (bf16[64,128]{1,0:T(8,128)(2,1)S(1)}, bf16[64,128]{1,0:T(8,128)(2,1)S(1)}, u32[]{:S(2)}, u32[]{:S(2)}) collective-permute-start(bf16[64,128]{1,0:T(8,128)(2,1)S(1)} %convert_element_type.64), channel_id=1, source_target_pairs={{0,6},{2,4},{4,2},{6,0},{1,7},{3,5},{5,3},{7,1},{8,14},{10,12},{12... | collective-permute-start | bytes 49160 | tf_op jit(solution)/shard_map/ppermute | solution.py:43
  75.4 0.3 collective-permute-start.1
  75.6 0.4 collective-permute-start
  76.1 0.4 collective-permute-done.2
  76.5 3.0 %collective-permute-done.1 = bf16[64,128]{1,0:T(8,128)(2,1)S(1)} collective-permute-done((bf16[64,128]{1,0:T(8,128)(2,1)S(1)}, bf16[64,128]{1,0:T(8,128)(2,1)S(1)}, u32[]{:S(2)}, u32[]{:S(2)}) %collective-permute-start.1) | collective-permute-done | bytes 16416 | tf_op jit(solution)/shard_map/ppermute | solution.py:43
  79.6 0.3 second_up.1
  79.8 18.5 %all_to_all.27 = bf16[16,72,128]{2,1,0:T(8,128)(2,1)S(1)} all-to-all(bf16[16,72,128]{2,1,0:T(8,128)(2,1)S(1)} %second_up.1), channel_id=1, replica_groups={{112,120,0,8,16,24,32,40,48,56,64,72,80,88,96,104},{113,121,1,9,17,25,3..., dimensions={0} | all-to-all | bytes 589824 | tf_op jit(solution)/shard_map/all_to_all | solution.py:28
  98.4 18.3 %all_to_all.28.everyone_ref = bf16[16,64,128]{2,1,0:T(8,128)(2,1)S(1)} all-to-all(bf16[16,64,128]{2,1,0:T(8,128)(2,1)S(1)} %broadcast_in_dim.25), channel_id=1, replica_groups={{112,120,0,8,16,24,32,40,48,56,64,72,80,88,96,104},{113,121,1,9,17,25,3..., dimensions={0} | all-to-all | bytes 524288 | tf_op jit(solution)/shard_map/all_to_all | solution.py:28
  116.8 0.2 down_sums.3
  117.0 1.1 collective-permute-start.5
  118.1 1.8 %collective-permute-start.4 = (bf16[64,128]{1,0:T(8,128)(2,1)S(1)}, bf16[64,128]{1,0:T(8,128)(2,1)S(1)}, u32[]{:S(2)}, u32[]{:S(2)}) collective-permute-start(bf16[64,128]{1,0:T(8,128)(2,1)S(1)} %convert_element_type.73), channel_id=1, source_target_pairs={{0,4},{2,6},{4,0},{6,2},{1,5},{3,7},{5,1},{7,3},{8,12},{10,14},{12... | collective-permute-start | bytes 49160 | tf_op jit(solution)/shard_map/ppermute | solution.py:43
  119.9 0.5 collective-permute-start.3
  120.4 0.5 collective-permute-done.5
  120.9 1.3 collective-permute-done.4
  122.2 0.3 collective-permute-done.3
  122.5 0.2 fusion
  122.7 13.4 %all_to_all.29 = f32[16,1,64]{2,1,0:T(1,128)S(1)} all-to-all(f32[16,1,64]{2,1,0:T(1,128)S(1)} %broadcast_in_dim.26), channel_id=1, replica_groups={{64,72,80,88,96,104,112,120,0,8,16,24,32,40,48,56},{65,73,81,89,97,105,..., dimensions={0} | all-to-all | bytes 8192 | tf_op jit(solution)/shard_map/all_to_all | solution.py:28
  136.1 0.7 fusion.2
  (30 shorter events, 0.4 us)
Async XLA Ops:
  14.6 25.9 %copy-start.4 = (f32[128]{0:T(128)S(1)}, f32[128]{0:T(128)}, u32[]{:S(2)}) copy-start(f32[128]{0:T(128)} %param.12) | copy-start | bytes 1540
  14.7 37.7 %all-to-all-start = ((bf16[16,72,128]{2,1,0:T(8,128)(2,1)}), bf16[16,72,128]{2,1,0:T(8,128)(2,1)S(1)}, u32[]{:S(2)}, u32[]{:S(2)}) async-start(bf16[16,72,128]{2,1,0:T(8,128)(2,1)} %first_up.1), calls=%async_computation | async-start | bytes 589824 | tf_op jit(solution)/shard_map/all_to_all | solution.py:28
  40.5 0.7 copy-start.5
  52.4 19.7 %copy-start = (bf16[2048,128]{1,0:T(8,128)(2,1)S(1)}, bf16[2048,128]{1,0:T(8,128)(2,1)}, u32[]{:S(2)}) copy-start(bf16[2048,128]{1,0:T(8,128)(2,1)} %down_ref.2) | copy-start | bytes 1572868
  72.1 7.5 %copy-start.1 = (bf16[128,2048]{1,0:T(8,128)(2,1)S(1)}, bf16[128,2048]{1,0:T(8,128)(2,1)}, u32[]{:S(2)}) copy-start(bf16[128,2048]{1,0:T(8,128)(2,1)} %up_ref.1) | copy-start | bytes 1572868
  72.3 7.1 %copy-start.3 = (bf16[64,128]{1,0:T(8,128)(2,1)S(1)}, bf16[64,128]{1,0:T(8,128)(2,1)}, u32[]{:S(2)}) copy-start(bf16[64,128]{1,0:T(8,128)(2,1)} %h_hbm.1) | copy-start | bytes 49156
  72.4 4.2 %collective-permute-start.2 = (bf16[64,128]{1,0:T(8,128)(2,1)S(1)}, bf16[64,128]{1,0:T(8,128)(2,1)S(1)}, u32[]{:S(2)}, u32[]{:S(2)}) collective-permute-start(bf16[64,128]{1,0:T(8,128)(2,1)S(1)} %convert_element_type.64), channel_id=1, source_target_pairs={{0,6},{2,4},{4,2},{6,0},{1,7},{3,5},{5,3},{7,1},{8,14},{10,12},{12... | collective-permute-start | bytes 49160 | tf_op jit(solution)/shard_map/ppermute | solution.py:43
  75.4 4.1 %collective-permute-start.1 = (bf16[64,128]{1,0:T(8,128)(2,1)S(1)}, bf16[64,128]{1,0:T(8,128)(2,1)S(1)}, u32[]{:S(2)}, u32[]{:S(2)}) collective-permute-start(bf16[64,128]{1,0:T(8,128)(2,1)S(1)} %convert_element_type.64), channel_id=1, source_target_pairs={{0,4},{2,6},{4,0},{6,2},{1,5},{3,7},{5,1},{7,3},{8,12},{10,14},{12... | collective-permute-start | bytes 49160 | tf_op jit(solution)/shard_map/ppermute | solution.py:43
  75.6 3.8 %collective-permute-start = (bf16[64,128]{1,0:T(8,128)(2,1)S(1)}, bf16[64,128]{1,0:T(8,128)(2,1)S(1)}, u32[]{:S(2)}, u32[]{:S(2)}) collective-permute-start(bf16[64,128]{1,0:T(8,128)(2,1)S(1)} %convert_element_type.64), channel_id=1, source_target_pairs={{0,2},{2,0},{4,6},{6,4},{1,3},{3,1},{5,7},{7,5},{8,10},{10,8},{12,... | collective-permute-start | bytes 49160 | tf_op jit(solution)/shard_map/ppermute | solution.py:43
  98.3 18.4 %copy-start.2 = (bf16[2048,128]{1,0:T(8,128)(2,1)S(1)}, bf16[2048,128]{1,0:T(8,128)(2,1)}, u32[]{:S(2)}) copy-start(bf16[2048,128]{1,0:T(8,128)(2,1)} %down_ref.3) | copy-start | bytes 1572868
  117.0 3.9 %collective-permute-start.5 = (bf16[64,128]{1,0:T(8,128)(2,1)S(1)}, bf16[64,128]{1,0:T(8,128)(2,1)S(1)}, u32[]{:S(2)}, u32[]{:S(2)}) collective-permute-start(bf16[64,128]{1,0:T(8,128)(2,1)S(1)} %convert_element_type.73), channel_id=1, source_target_pairs={{0,6},{2,4},{4,2},{6,0},{1,7},{3,5},{5,3},{7,1},{8,14},{10,12},{12... | collective-permute-start | bytes 49160 | tf_op jit(solution)/shard_map/ppermute | solution.py:43
  118.1 4.1 %collective-permute-start.4 = (bf16[64,128]{1,0:T(8,128)(2,1)S(1)}, bf16[64,128]{1,0:T(8,128)(2,1)S(1)}, u32[]{:S(2)}, u32[]{:S(2)}) collective-permute-start(bf16[64,128]{1,0:T(8,128)(2,1)S(1)} %convert_element_type.73), channel_id=1, source_target_pairs={{0,4},{2,6},{4,0},{6,2},{1,5},{3,7},{5,1},{7,3},{8,12},{10,14},{12... | collective-permute-start | bytes 49160 | tf_op jit(solution)/shard_map/ppermute | solution.py:43
  119.9 2.6 %collective-permute-start.3 = (bf16[64,128]{1,0:T(8,128)(2,1)S(1)}, bf16[64,128]{1,0:T(8,128)(2,1)S(1)}, u32[]{:S(2)}, u32[]{:S(2)}) collective-permute-start(bf16[64,128]{1,0:T(8,128)(2,1)S(1)} %convert_element_type.73), channel_id=1, source_target_pairs={{0,2},{2,0},{4,6},{6,4},{1,3},{3,1},{5,7},{7,5},{8,10},{10,8},{12,... | collective-permute-start | bytes 49160 | tf_op jit(solution)/shard_map/ppermute | solution.py:43

commit v8 on v7

--- a/solution.py
+++ b/solution.py
@@ -15,7 +15,7 @@
 SUM_TYPE = BF16
 UP_COST = 2 << 20
 PAD = 8
-CHUNKS = 2
+CHUNKS = 1
 
 
 def member_order(size, eighths=None):

time: 137 us -> 138 us (level)
  transfers between devices with their start and end apart: 7 -> 7, of which waited for: 6 -> 5; matrix products, arithmetic and copies ran while one was open for 0% -> 0% of each run, Pallas kernels for 0% -> 0%
where the time goes in v8:
time: 138 us
  blocking collectives  70.5 us (51%)
  starting transfers between devices  33 us (24%)
  waiting for transfers between devices  16.8 us (12%)
  Pallas kernels  15.2 us (11%)
    all_to_all x4, blocking collectives, exchange(): lax.all_to_all(pieces, 'ra', split_axis=0, concat_axis=0, tiled=True, axi...  70.5 us
    all_to_all x1, starting transfers between devices, exchange(): lax.all_to_all(pieces, 'ra', split_axis=0, concat_axis=0, tiled=True, axi...  25.9 us
    pallas_call x1, Pallas kernels, first_up(): pl.pallas_call(first_up_body, out_shape=pieces, in_specs=[hbm] * 3, out_s...  14.5 us
    all_to_all x1, waiting for transfers between devices, exchange(): lax.all_to_all(pieces, 'ra', split_axis=0, concat_axis=0, tiled=True, axi...  11.2 us
    ppermute x6, starting transfers between devices, summed_over(): total = total + lax.ppermute(sent, axis, pairs).astype(F32)  7.11 us
    ppermute x6, waiting for transfers between devices, summed_over(): total = total + lax.ppermute(sent, axis, pairs).astype(F32)  5.6 us
  transfers between devices with their start and end apart: 7, of which 5 were waited for; matrix products, arithmetic and copies ran while one was open for 0% of the time, Pallas kernels for 0%

profile of v8, /device:TPU:33, one launch (start us, length us, event | category | flops | bytes accessed | tf_op | source)
XLA Modules:
  0.0 137.5 jit_solution(15878330449764763073)
XLA Ops:
  0.0 14.5 %first_up.1 = bf16[16,72,128]{2,1,0:T(8,128)(2,1)} custom-call(bf16[64,128]{1,0:T(8,128)(2,1)} %h_hbm.1, f32[1,128]{1,0:T(1,128)} %bitcast.3, bf16[128,2048]{1,0:T(8,128)(2,1)} %up_hbm.1), custom_call_target="tpu_custom_call" | custom-call | flops 33554432 | bytes 2097152 | tf_op jit(solution)/shard_map/first_up/pallas_call | solution.py:135
  14.5 25.9 %all-to-all-start = ((bf16[16,72,128]{2,1,0:T(8,128)(2,1)}), bf16[16,72,128]{2,1,0:T(8,128)(2,1)S(1)}, u32[]{:S(2)}, u32[]{:S(2)}) async-start(bf16[16,72,128]{2,1,0:T(8,128)(2,1)} %first_up.1), calls=%async_computation | async-start | bytes 589824 | tf_op jit(solution)/shard_map/all_to_all | solution.py:28
  40.4 0.6 copy-done.5
  41.0 11.2 %all-to-all-done = bf16[16,72,128]{2,1,0:T(8,128)(2,1)S(1)} async-done(((bf16[16,72,128]{2,1,0:T(8,128)(2,1)}), bf16[16,72,128]{2,1,0:T(8,128)(2,1)S(1)}, u32[]{:S(2)}, u32[]{:S(2)}) %all-to-all-start) | async-done | bytes 294944 | tf_op jit(solution)/shard_map/all_to_all | solution.py:28
  52.4 19.6 %all_to_all.26.everyone_ref = bf16[16,64,128]{2,1,0:T(8,128)(2,1)S(1)} all-to-all(bf16[16,64,128]{2,1,0:T(8,128)(2,1)S(1)} %broadcast_in_dim.24), channel_id=1, replica_groups={{112,120,0,8,16,24,32,40,48,56,64,72,80,88,96,104},{113,121,1,9,17,25,3..., dimensions={0} | all-to-all | bytes 524288 | tf_op jit(solution)/shard_map/all_to_all | solution.py:28
  72.0 0.2 down_sums.2
  72.2 3.0 %collective-permute-start.2 = (bf16[64,128]{1,0:T(8,128)(2,1)S(1)}, bf16[64,128]{1,0:T(8,128)(2,1)S(1)}, u32[]{:S(2)}, u32[]{:S(2)}) collective-permute-start(bf16[64,128]{1,0:T(8,128)(2,1)S(1)} %convert_element_type.64), channel_id=1, source_target_pairs={{0,6},{2,4},{4,2},{6,0},{1,7},{3,5},{5,3},{7,1},{8,14},{10,12},{12... | collective-permute-start | bytes 49160 | tf_op jit(solution)/shard_map/ppermute | solution.py:43
  75.2 0.3 collective-permute-start.1
  75.5 0.5 collective-permute-start
  76.0 0.4 collective-permute-done.2
  76.4 3.0 %collective-permute-done.1 = bf16[64,128]{1,0:T(8,128)(2,1)S(1)} collective-permute-done((bf16[64,128]{1,0:T(8,128)(2,1)S(1)}, bf16[64,128]{1,0:T(8,128)(2,1)S(1)}, u32[]{:S(2)}, u32[]{:S(2)}) %collective-permute-start.1) | collective-permute-done | bytes 16416 | tf_op jit(solution)/shard_map/ppermute | solution.py:43
  79.3 0.1 add_convert_fusion.1.h_ref
  79.4 0.3 second_up.1
  79.7 18.5 %all_to_all.27 = bf16[16,72,128]{2,1,0:T(8,128)(2,1)S(1)} all-to-all(bf16[16,72,128]{2,1,0:T(8,128)(2,1)S(1)} %second_up.1), channel_id=1, replica_groups={{112,120,0,8,16,24,32,40,48,56,64,72,80,88,96,104},{113,121,1,9,17,25,3..., dimensions={0} | all-to-all | bytes 589824 | tf_op jit(solution)/shard_map/all_to_all | solution.py:28
  98.3 18.4 %all_to_all.28.everyone_ref = bf16[16,64,128]{2,1,0:T(8,128)(2,1)S(1)} all-to-all(bf16[16,64,128]{2,1,0:T(8,128)(2,1)S(1)} %broadcast_in_dim.25), channel_id=1, replica_groups={{112,120,0,8,16,24,32,40,48,56,64,72,80,88,96,104},{113,121,1,9,17,25,3..., dimensions={0} | all-to-all | bytes 524288 | tf_op jit(solution)/shard_map/all_to_all | solution.py:28
  116.7 0.2 down_sums.3
  117.0 1.5 %collective-permute-start.5 = (bf16[64,128]{1,0:T(8,128)(2,1)S(1)}, bf16[64,128]{1,0:T(8,128)(2,1)S(1)}, u32[]{:S(2)}, u32[]{:S(2)}) collective-permute-start(bf16[64,128]{1,0:T(8,128)(2,1)S(1)} %convert_element_type.73), channel_id=1, source_target_pairs={{0,6},{2,4},{4,2},{6,0},{1,7},{3,5},{5,3},{7,1},{8,14},{10,12},{12... | collective-permute-start | bytes 49160 | tf_op jit(solution)/shard_map/ppermute | solution.py:43
  118.5 0.9 collective-permute-start.4
  119.4 0.9 collective-permute-start.3
  120.4 0.5 collective-permute-done.5
  120.9 1.7 %collective-permute-done.4 = bf16[64,128]{1,0:T(8,128)(2,1)S(1)} collective-permute-done((bf16[64,128]{1,0:T(8,128)(2,1)S(1)}, bf16[64,128]{1,0:T(8,128)(2,1)S(1)}, u32[]{:S(2)}, u32[]{:S(2)}) %collective-permute-start.4) | collective-permute-done | bytes 16416 | tf_op jit(solution)/shard_map/ppermute | solution.py:43
  122.6 0.2 fusion
  122.8 14.0 %all_to_all.29 = f32[16,1,64]{2,1,0:T(1,128)S(1)} all-to-all(f32[16,1,64]{2,1,0:T(1,128)S(1)} %broadcast_in_dim.26), channel_id=1, replica_groups={{64,72,80,88,96,104,112,120,0,8,16,24,32,40,48,56},{65,73,81,89,97,105,..., dimensions={0} | all-to-all | bytes 8192 | tf_op jit(solution)/shard_map/all_to_all | solution.py:28
  136.8 0.7 fusion.2
  (30 shorter events, 0.4 us)
Async XLA Ops:
  14.5 25.9 %copy-start.4 = (f32[128]{0:T(128)S(1)}, f32[128]{0:T(128)}, u32[]{:S(2)}) copy-start(f32[128]{0:T(128)} %param.12) | copy-start | bytes 1540
  14.5 37.7 %all-to-all-start = ((bf16[16,72,128]{2,1,0:T(8,128)(2,1)}), bf16[16,72,128]{2,1,0:T(8,128)(2,1)S(1)}, u32[]{:S(2)}, u32[]{:S(2)}) async-start(bf16[16,72,128]{2,1,0:T(8,128)(2,1)} %first_up.1), calls=%async_computation | async-start | bytes 589824 | tf_op jit(solution)/shard_map/all_to_all | solution.py:28
  40.4 0.7 copy-start.5
  52.2 19.7 %copy-start = (bf16[2048,128]{1,0:T(8,128)(2,1)S(1)}, bf16[2048,128]{1,0:T(8,128)(2,1)}, u32[]{:S(2)}) copy-start(bf16[2048,128]{1,0:T(8,128)(2,1)} %down_ref.2) | copy-start | bytes 1572868
  72.0 7.5 %copy-start.1 = (bf16[128,2048]{1,0:T(8,128)(2,1)S(1)}, bf16[128,2048]{1,0:T(8,128)(2,1)}, u32[]{:S(2)}) copy-start(bf16[128,2048]{1,0:T(8,128)(2,1)} %up_ref.1) | copy-start | bytes 1572868
  72.2 7.1 %copy-start.3 = (bf16[64,128]{1,0:T(8,128)(2,1)S(1)}, bf16[64,128]{1,0:T(8,128)(2,1)}, u32[]{:S(2)}) copy-start(bf16[64,128]{1,0:T(8,128)(2,1)} %h_hbm.1) | copy-start | bytes 49156
  72.2 4.2 %collective-permute-start.2 = (bf16[64,128]{1,0:T(8,128)(2,1)S(1)}, bf16[64,128]{1,0:T(8,128)(2,1)S(1)}, u32[]{:S(2)}, u32[]{:S(2)}) collective-permute-start(bf16[64,128]{1,0:T(8,128)(2,1)S(1)} %convert_element_type.64), channel_id=1, source_target_pairs={{0,6},{2,4},{4,2},{6,0},{1,7},{3,5},{5,3},{7,1},{8,14},{10,12},{12... | collective-permute-start | bytes 49160 | tf_op jit(solution)/shard_map/ppermute | solution.py:43
  75.2 4.1 %collective-permute-start.1 = (bf16[64,128]{1,0:T(8,128)(2,1)S(1)}, bf16[64,128]{1,0:T(8,128)(2,1)S(1)}, u32[]{:S(2)}, u32[]{:S(2)}) collective-permute-start(bf16[64,128]{1,0:T(8,128)(2,1)S(1)} %convert_element_type.64), channel_id=1, source_target_pairs={{0,4},{2,6},{4,0},{6,2},{1,5},{3,7},{5,1},{7,3},{8,12},{10,14},{12... | collective-permute-start | bytes 49160 | tf_op jit(solution)/shard_map/ppermute | solution.py:43
  75.5 3.8 %collective-permute-start = (bf16[64,128]{1,0:T(8,128)(2,1)S(1)}, bf16[64,128]{1,0:T(8,128)(2,1)S(1)}, u32[]{:S(2)}, u32[]{:S(2)}) collective-permute-start(bf16[64,128]{1,0:T(8,128)(2,1)S(1)} %convert_element_type.64), channel_id=1, source_target_pairs={{0,2},{2,0},{4,6},{6,4},{1,3},{3,1},{5,7},{7,5},{8,10},{10,8},{12,... | collective-permute-start | bytes 49160 | tf_op jit(solution)/shard_map/ppermute | solution.py:43
  98.2 18.5 %copy-start.2 = (bf16[2048,128]{1,0:T(8,128)(2,1)S(1)}, bf16[2048,128]{1,0:T(8,128)(2,1)}, u32[]{:S(2)}) copy-start(bf16[2048,128]{1,0:T(8,128)(2,1)} %down_ref.3) | copy-start | bytes 1572868
  117.0 3.9 %collective-permute-start.5 = (bf16[64,128]{1,0:T(8,128)(2,1)S(1)}, bf16[64,128]{1,0:T(8,128)(2,1)S(1)}, u32[]{:S(2)}, u32[]{:S(2)}) collective-permute-start(bf16[64,128]{1,0:T(8,128)(2,1)S(1)} %convert_element_type.73), channel_id=1, source_target_pairs={{0,6},{2,4},{4,2},{6,0},{1,7},{3,5},{5,3},{7,1},{8,14},{10,12},{12... | collective-permute-start | bytes 49160 | tf_op jit(solution)/shard_map/ppermute | solution.py:43
  118.5 4.1 %collective-permute-start.4 = (bf16[64,128]{1,0:T(8,128)(2,1)S(1)}, bf16[64,128]{1,0:T(8,128)(2,1)S(1)}, u32[]{:S(2)}, u32[]{:S(2)}) collective-permute-start(bf16[64,128]{1,0:T(8,128)(2,1)S(1)} %convert_element_type.73), channel_id=1, source_target_pairs={{0,4},{2,6},{4,0},{6,2},{1,5},{3,7},{5,1},{7,3},{8,12},{10,14},{12... | collective-permute-start | bytes 49160 | tf_op jit(solution)/shard_map/ppermute | solution.py:43
  119.4 3.2 %collective-permute-start.3 = (bf16[64,128]{1,0:T(8,128)(2,1)S(1)}, bf16[64,128]{1,0:T(8,128)(2,1)S(1)}, u32[]{:S(2)}, u32[]{:S(2)}) collective-permute-start(bf16[64,128]{1,0:T(8,128)(2,1)S(1)} %convert_element_type.73), channel_id=1, source_target_pairs={{0,2},{2,0},{4,6},{6,4},{1,3},{3,1},{5,7},{7,5},{8,10},{10,8},{12,... | collective-permute-start | bytes 49160 | tf_op jit(solution)/shard_map/ppermute | solution.py:43

commit v9 on v7

--- a/solution.py
+++ b/solution.py
@@ -11,7 +11,7 @@
 STAGGER_NS = 13300
 STAGGER_CORE = 1
 LEAD_EIGHTHS = 7
-LAST_LEAD_EIGHTHS = 4
+LAST_LEAD_EIGHTHS = 5
 SUM_TYPE = BF16
 UP_COST = 2 << 20
 PAD = 8

time: 137 us -> 138 us (level)
  no operation moved by 1% of the time
where the time goes in v9:
time: 138 us
  blocking collectives  70.6 us (51%)
  starting transfers between devices  33 us (24%)
  waiting for transfers between devices  16.7 us (12%)
  Pallas kernels  15.3 us (11%)
    all_to_all x4, blocking collectives, exchange(): lax.all_to_all(pieces, 'ra', split_axis=0, concat_axis=0, tiled=True, axi...  70.6 us
    all_to_all x1, starting transfers between devices, exchange(): lax.all_to_all(pieces, 'ra', split_axis=0, concat_axis=0, tiled=True, axi...  25.9 us
    pallas_call x1, Pallas kernels, first_up(): pl.pallas_call(first_up_body, out_shape=pieces, in_specs=[hbm] * 3, out_s...  14.6 us
    all_to_all x1, waiting for transfers between devices, exchange(): lax.all_to_all(pieces, 'ra', split_axis=0, concat_axis=0, tiled=True, axi...  11.2 us
    ppermute x6, starting transfers between devices, summed_over(): total = total + lax.ppermute(sent, axis, pairs).astype(F32)  7.11 us
    ppermute x6, waiting for transfers between devices, summed_over(): total = total + lax.ppermute(sent, axis, pairs).astype(F32)  5.49 us
  transfers between devices with their start and end apart: 7, of which 6 were waited for; matrix products, arithmetic and copies ran while one was open for 0% of the time, Pallas kernels for 0%

profile of v9, /device:TPU:33, one launch (start us, length us, event | category | flops | bytes accessed | tf_op | source)
XLA Modules:
  0.0 137.7 jit_solution(2205574438283990797)
XLA Ops:
  0.0 14.6 %first_up.1 = bf16[16,72,128]{2,1,0:T(8,128)(2,1)} custom-call(bf16[64,128]{1,0:T(8,128)(2,1)} %h_hbm.1, f32[1,128]{1,0:T(1,128)} %bitcast.3, bf16[128,2048]{1,0:T(8,128)(2,1)} %up_hbm.1), custom_call_target="tpu_custom_call" | custom-call | flops 33554432 | bytes 2097152 | tf_op jit(solution)/shard_map/first_up/pallas_call | solution.py:135
  14.7 25.9 %all-to-all-start = ((bf16[16,72,128]{2,1,0:T(8,128)(2,1)}), bf16[16,72,128]{2,1,0:T(8,128)(2,1)S(1)}, u32[]{:S(2)}, u32[]{:S(2)}) async-start(bf16[16,72,128]{2,1,0:T(8,128)(2,1)} %first_up.1), calls=%async_computation | async-start | bytes 589824 | tf_op jit(solution)/shard_map/all_to_all | solution.py:28
  40.5 0.6 copy-done.5
  41.2 11.2 %all-to-all-done = bf16[16,72,128]{2,1,0:T(8,128)(2,1)S(1)} async-done(((bf16[16,72,128]{2,1,0:T(8,128)(2,1)}), bf16[16,72,128]{2,1,0:T(8,128)(2,1)S(1)}, u32[]{:S(2)}, u32[]{:S(2)}) %all-to-all-start) | async-done | bytes 294944 | tf_op jit(solution)/shard_map/all_to_all | solution.py:28
  52.5 19.6 %all_to_all.26.everyone_ref = bf16[16,64,128]{2,1,0:T(8,128)(2,1)S(1)} all-to-all(bf16[16,64,128]{2,1,0:T(8,128)(2,1)S(1)} %broadcast_in_dim.24), channel_id=1, replica_groups={{112,120,0,8,16,24,32,40,48,56,64,72,80,88,96,104},{113,121,1,9,17,25,3..., dimensions={0} | all-to-all | bytes 524288 | tf_op jit(solution)/shard_map/all_to_all | solution.py:28
  72.1 0.2 down_sums.2
  72.4 3.0 %collective-permute-start.2 = (bf16[64,128]{1,0:T(8,128)(2,1)S(1)}, bf16[64,128]{1,0:T(8,128)(2,1)S(1)}, u32[]{:S(2)}, u32[]{:S(2)}) collective-permute-start(bf16[64,128]{1,0:T(8,128)(2,1)S(1)} %convert_element_type.64), channel_id=1, source_target_pairs={{0,6},{2,4},{4,2},{6,0},{1,7},{3,5},{5,3},{7,1},{8,14},{10,12},{12... | collective-permute-start | bytes 49160 | tf_op jit(solution)/shard_map/ppermute | solution.py:43
  75.4 0.3 collective-permute-start.1
  75.6 0.4 collective-permute-start
  76.1 0.4 collective-permute-done.2
  76.5 3.0 %collective-permute-done.1 = bf16[64,128]{1,0:T(8,128)(2,1)S(1)} collective-permute-done((bf16[64,128]{1,0:T(8,128)(2,1)S(1)}, bf16[64,128]{1,0:T(8,128)(2,1)S(1)}, u32[]{:S(2)}, u32[]{:S(2)}) %collective-permute-start.1) | collective-permute-done | bytes 16416 | tf_op jit(solution)/shard_map/ppermute | solution.py:43
  79.6 0.3 second_up.1
  79.8 18.5 %all_to_all.27 = bf16[16,72,128]{2,1,0:T(8,128)(2,1)S(1)} all-to-all(bf16[16,72,128]{2,1,0:T(8,128)(2,1)S(1)} %second_up.1), channel_id=1, replica_groups={{112,120,0,8,16,24,32,40,48,56,64,72,80,88,96,104},{113,121,1,9,17,25,3..., dimensions={0} | all-to-all | bytes 589824 | tf_op jit(solution)/shard_map/all_to_all | solution.py:28
  98.4 18.3 %all_to_all.28.everyone_ref = bf16[16,64,128]{2,1,0:T(8,128)(2,1)S(1)} all-to-all(bf16[16,64,128]{2,1,0:T(8,128)(2,1)S(1)} %broadcast_in_dim.25), channel_id=1, replica_groups={{112,120,0,8,16,24,32,40,48,56,64,72,80,88,96,104},{113,121,1,9,17,25,3..., dimensions={0} | all-to-all | bytes 524288 | tf_op jit(solution)/shard_map/all_to_all | solution.py:28
  116.8 0.2 down_sums.3
  117.0 1.1 collective-permute-start.5
  118.1 1.8 %collective-permute-start.4 = (bf16[64,128]{1,0:T(8,128)(2,1)S(1)}, bf16[64,128]{1,0:T(8,128)(2,1)S(1)}, u32[]{:S(2)}, u32[]{:S(2)}) collective-permute-start(bf16[64,128]{1,0:T(8,128)(2,1)S(1)} %convert_element_type.73), channel_id=1, source_target_pairs={{0,4},{2,6},{4,0},{6,2},{1,5},{3,7},{5,1},{7,3},{8,12},{10,14},{12... | collective-permute-start | bytes 49160 | tf_op jit(solution)/shard_map/ppermute | solution.py:43
  119.9 0.5 collective-permute-start.3
  120.4 0.5 collective-permute-done.5
  120.9 1.3 collective-permute-done.4
  122.2 0.3 collective-permute-done.3
  122.5 0.2 fusion
  122.7 14.3 %all_to_all.29 = f32[16,1,64]{2,1,0:T(1,128)S(1)} all-to-all(f32[16,1,64]{2,1,0:T(1,128)S(1)} %broadcast_in_dim.26), channel_id=1, replica_groups={{80,88,96,104,112,120,0,8,16,24,32,40,48,56,64,72},{81,89,97,105,113,12..., dimensions={0} | all-to-all | bytes 8192 | tf_op jit(solution)/shard_map/all_to_all | solution.py:28
  137.0 0.7 fusion.2
  (30 shorter events, 0.4 us)
Async XLA Ops:
  14.6 25.9 %copy-start.4 = (f32[128]{0:T(128)S(1)}, f32[128]{0:T(128)}, u32[]{:S(2)}) copy-start(f32[128]{0:T(128)} %param.12) | copy-start | bytes 1540
  14.7 37.7 %all-to-all-start = ((bf16[16,72,128]{2,1,0:T(8,128)(2,1)}), bf16[16,72,128]{2,1,0:T(8,128)(2,1)S(1)}, u32[]{:S(2)}, u32[]{:S(2)}) async-start(bf16[16,72,128]{2,1,0:T(8,128)(2,1)} %first_up.1), calls=%async_computation | async-start | bytes 589824 | tf_op jit(solution)/shard_map/all_to_all | solution.py:28
  40.5 0.7 copy-start.5
  52.4 19.7 %copy-start = (bf16[2048,128]{1,0:T(8,128)(2,1)S(1)}, bf16[2048,128]{1,0:T(8,128)(2,1)}, u32[]{:S(2)}) copy-start(bf16[2048,128]{1,0:T(8,128)(2,1)} %down_ref.2) | copy-start | bytes 1572868
  72.1 7.5 %copy-start.1 = (bf16[128,2048]{1,0:T(8,128)(2,1)S(1)}, bf16[128,2048]{1,0:T(8,128)(2,1)}, u32[]{:S(2)}) copy-start(bf16[128,2048]{1,0:T(8,128)(2,1)} %up_ref.1) | copy-start | bytes 1572868
  72.3 7.1 %copy-start.3 = (bf16[64,128]{1,0:T(8,128)(2,1)S(1)}, bf16[64,128]{1,0:T(8,128)(2,1)}, u32[]{:S(2)}) copy-start(bf16[64,128]{1,0:T(8,128)(2,1)} %h_hbm.1) | copy-start | bytes 49156
  72.4 4.2 %collective-permute-start.2 = (bf16[64,128]{1,0:T(8,128)(2,1)S(1)}, bf16[64,128]{1,0:T(8,128)(2,1)S(1)}, u32[]{:S(2)}, u32[]{:S(2)}) collective-permute-start(bf16[64,128]{1,0:T(8,128)(2,1)S(1)} %convert_element_type.64), channel_id=1, source_target_pairs={{0,6},{2,4},{4,2},{6,0},{1,7},{3,5},{5,3},{7,1},{8,14},{10,12},{12... | collective-permute-start | bytes 49160 | tf_op jit(solution)/shard_map/ppermute | solution.py:43
  75.4 4.1 %collective-permute-start.1 = (bf16[64,128]{1,0:T(8,128)(2,1)S(1)}, bf16[64,128]{1,0:T(8,128)(2,1)S(1)}, u32[]{:S(2)}, u32[]{:S(2)}) collective-permute-start(bf16[64,128]{1,0:T(8,128)(2,1)S(1)} %convert_element_type.64), channel_id=1, source_target_pairs={{0,4},{2,6},{4,0},{6,2},{1,5},{3,7},{5,1},{7,3},{8,12},{10,14},{12... | collective-permute-start | bytes 49160 | tf_op jit(solution)/shard_map/ppermute | solution.py:43
  75.6 3.8 %collective-permute-start = (bf16[64,128]{1,0:T(8,128)(2,1)S(1)}, bf16[64,128]{1,0:T(8,128)(2,1)S(1)}, u32[]{:S(2)}, u32[]{:S(2)}) collective-permute-start(bf16[64,128]{1,0:T(8,128)(2,1)S(1)} %convert_element_type.64), channel_id=1, source_target_pairs={{0,2},{2,0},{4,6},{6,4},{1,3},{3,1},{5,7},{7,5},{8,10},{10,8},{12,... | collective-permute-start | bytes 49160 | tf_op jit(solution)/shard_map/ppermute | solution.py:43
  98.3 18.4 %copy-start.2 = (bf16[2048,128]{1,0:T(8,128)(2,1)S(1)}, bf16[2048,128]{1,0:T(8,128)(2,1)}, u32[]{:S(2)}) copy-start(bf16[2048,128]{1,0:T(8,128)(2,1)} %down_ref.3) | copy-start | bytes 1572868
  117.0 3.9 %collective-permute-start.5 = (bf16[64,128]{1,0:T(8,128)(2,1)S(1)}, bf16[64,128]{1,0:T(8,128)(2,1)S(1)}, u32[]{:S(2)}, u32[]{:S(2)}) collective-permute-start(bf16[64,128]{1,0:T(8,128)(2,1)S(1)} %convert_element_type.73), channel_id=1, source_target_pairs={{0,6},{2,4},{4,2},{6,0},{1,7},{3,5},{5,3},{7,1},{8,14},{10,12},{12... | collective-permute-start | bytes 49160 | tf_op jit(solution)/shard_map/ppermute | solution.py:43
  118.1 4.1 %collective-permute-start.4 = (bf16[64,128]{1,0:T(8,128)(2,1)S(1)}, bf16[64,128]{1,0:T(8,128)(2,1)S(1)}, u32[]{:S(2)}, u32[]{:S(2)}) collective-permute-start(bf16[64,128]{1,0:T(8,128)(2,1)S(1)} %convert_element_type.73), channel_id=1, source_target_pairs={{0,4},{2,6},{4,0},{6,2},{1,5},{3,7},{5,1},{7,3},{8,12},{10,14},{12... | collective-permute-start | bytes 49160 | tf_op jit(solution)/shard_map/ppermute | solution.py:43
  119.9 2.6 %collective-permute-start.3 = (bf16[64,128]{1,0:T(8,128)(2,1)S(1)}, bf16[64,128]{1,0:T(8,128)(2,1)S(1)}, u32[]{:S(2)}, u32[]{:S(2)}) collective-permute-start(bf16[64,128]{1,0:T(8,128)(2,1)S(1)} %convert_element_type.73), channel_id=1, source_target_pairs={{0,2},{2,0},{4,6},{6,4},{1,3},{3,1},{5,7},{7,5},{8,10},{10,8},{12,... | collective-permute-start | bytes 49160 | tf_op jit(solution)/shard_map/ppermute | solution.py:43
